TPU v7x, 32 devices: a whole 2x2x4 slice. The times are simulated.
32 devices in a mesh: fs: 4 (over z), rep: 4 (over y, x), tp: 2 (over core).
Axes of the slice: x: 2, y: 2, z: 4, core: 2. Of those that a mesh axis runs over, the one named last changes fastest.
Arguments:
- saved_input: bfloat16 [5632, 2048], P(('fs', 'rep')), may hold values from -6 to 6
- query_cot: bfloat16 [5632, 1024], P(('fs', 'rep'), 'tp'), may hold values from -0.078125 to 0.078125
- attn_out: bfloat16 [5632, 1024], P(('fs', 'rep'), 'tp'), may hold values from -6 to 6
- out_cot: bfloat16 [5632, 2048], P(('fs', 'rep')), may hold values from -0.078125 to 0.078125
- query_basis: bfloat16 [2048, 512], P('fs'), may hold values from -0.25 to 0.25
- output_basis: bfloat16 [2048, 512], P('fs'), may hold values from -0.25 to 0.25
- query_weight: float32 [2048, 1024], P('fs', 'tp'), may hold values from -6 to 6
- output_weight: float32 [1024, 2048], P('tp', 'fs'), may hold values from -6 to 6
- query_moment: float32 [512, 1024], P('rep', 'tp'), may hold values from -52 to 52
- output_moment: float32 [1024, 512], P('tp', 'rep'), may hold values from -52 to 52
Outputs:
- query_step: float32 [2048, 1024], P('fs', 'tp')
- output_step: float32 [1024, 2048], P('tp', 'fs')
- query_new: float32 [2048, 1024], P('fs', 'tp')
- output_new: float32 [1024, 2048], P('tp', 'fs')
- query_copy: bfloat16 [2048, 1024], P('fs', 'tp')
- output_copy: bfloat16 [1024, 2048], P('tp', 'fs')
- query_moment_new: float32 [512, 1024], P('rep', 'tp')
- output_moment_new: float32 [1024, 512], P('tp', 'rep')
All inputs are finite; a program needn't handle non-finite values.
Results may differ from a plain program's by a relative error of at most 0.0029.
Values may be sent and summed in bfloat16 or wider, within the bound.
A program may use at most 64 MiB of HBM per device.

v0:
```python
import functools

import jax
import jax.numpy as jnp
from jax import lax
from jax.experimental import pallas as pl
from jax.experimental.pallas import tpu as pltpu
from jax.sharding import PartitionSpec as P

BETA = 0.8
RATE = 0.2
EPS = 1e-06


def on_device(
    saved_input,
    query_cot,
    attn_out,
    out_cot,
    query_basis,
    output_basis,
    query_weight,
    output_weight,
    query_moment,
    output_moment,
):
    rank = query_basis.shape[1]
    grad_rows = lax.psum_scatter(
        jnp.dot(saved_input.T, query_cot, preferred_element_type=jnp.float32),
        "fs",
        scatter_dimension=0,
        tiled=True,
    )
    query_part = jnp.dot(
        query_basis.astype(jnp.float32).T, grad_rows, precision=lax.Precision.HIGHEST
    )
    cot_proj = jnp.dot(
        out_cot,
        lax.all_gather(output_basis, "fs", axis=0, tiled=True),
        preferred_element_type=jnp.float32,
    )
    output_part = jnp.dot(attn_out.astype(jnp.float32).T, cot_proj, precision=lax.Precision.HIGHEST)
    reps = lax.axis_size("rep")
    share = rank // reps
    query_terms, output_terms = (
        lax.all_to_all(
            query_part.astype(jnp.bfloat16), "rep", split_axis=0, concat_axis=0, tiled=True
        ).astype(query_part.dtype),
        lax.all_to_all(
            output_part.T.astype(jnp.bfloat16), "rep", split_axis=0, concat_axis=0, tiled=True
        ).astype(jnp.float32),
    )
    width = query_part.shape[1]
    query_local = jnp.sum(query_terms.reshape(reps, share, width), axis=0)
    output_local = jnp.sum(output_terms.reshape(reps, share, width), axis=0)
    query_share, output_flip = lax.psum((query_local, output_local), "fs")
    output_share = output_flip.T
    query_moment_new = BETA * query_moment + (1.0 - BETA) * query_share
    output_moment_new = BETA * output_moment + (1.0 - BETA) * output_share
    query_squares, output_squares = lax.psum(
        (
            jnp.sum(query_moment_new * query_moment_new),
            jnp.sum(output_moment_new * output_moment_new),
        ),
        ("rep", "tp"),
    )
    entries = rank * query_moment.shape[1] * lax.axis_size("tp")
    query_dir = (query_moment_new * lax.rsqrt(query_squares / entries + EPS)).astype(jnp.bfloat16)
    output_dir = (output_moment_new * lax.rsqrt(output_squares / entries + EPS)).astype(
        jnp.bfloat16
    )
    query_full, output_full = (
        lax.all_gather(query_dir, "rep", axis=0, tiled=True),
        lax.all_gather(output_dir, "rep", axis=1, tiled=True),
    )
    query_step = jnp.dot(query_basis, query_full, preferred_element_type=jnp.float32)
    output_step = jnp.dot(output_full, output_basis.T, preferred_element_type=jnp.float32)
    query_new = query_weight - RATE * query_step
    output_new = output_weight - RATE * output_step
    return (
        query_step,
        output_step,
        query_new,
        output_new,
        query_new.astype(jnp.bfloat16),
        output_new.astype(jnp.bfloat16),
        query_moment_new,
        output_moment_new,
    )


MESH = pl.DeviceIdType.MESH
CHUNKS = 2


def exchange_kernel(
    entries,
    si_hbm, oc_hbm, qc_hbm, ao_hbm, qb_hbm, ob_hbm, mq_hbm, mo_hbm,
    full_out, mom_out,
    act, cot, base, mq, mo, gath, xb, pb, t1, sb, t2, ag, mom, nrm, full,
    load_sem, store_sem, az_s, az_r, aw_s, aw_r, xc_s, xc_r,
    b1_s, b1_r, b2_s, b2_r, g_s, g_r, n_s, n_r, d_s, d_r,
):
    f, r, t = lax.axis_index("fs"), lax.axis_index("rep"), lax.axis_index("tp")
    y, x = r // 2, r % 2
    ot = 1 - t
    fpeer = [(f + d) % 4 for d in (1, 3, 2)]
    fsrc = [(f + 4 - d) % 4 for d in (1, 3, 2)]
    rpeer = [2 * y + (1 - x), 2 * (1 - y) + x, 3 - r]
    depth, rank = base.shape[1], base.shape[2]
    hd, hr = depth // 2, rank // 2
    share = rank // 4

    loads = []
    for k, (src, dst) in enumerate((
        (qb_hbm, base.at[0]), (ob_hbm, base.at[1]), (si_hbm, act.at[0]), (oc_hbm, act.at[1]),
        (qc_hbm, cot.at[0]), (ao_hbm, cot.at[1]), (mq_hbm, mq), (mo_hbm, mo),
    )):
        c = pltpu.make_async_copy(src, dst, load_sem.at[k])
        c.start()
        loads.append(c)

    barrier = pltpu.get_barrier_semaphore()
    for g in fpeer:
        pl.semaphore_signal(barrier, inc=1, device_id=(g, r, t), device_id_type=MESH)
    for q in rpeer:
        for s in (t, ot):
            pl.semaphore_signal(barrier, inc=1, device_id=(f, q, s), device_id_type=MESH)
    pl.semaphore_signal(barrier, inc=1, device_id=(f, r, ot), device_id_type=MESH)
    pl.semaphore_wait(barrier, 10)

    def remote(src, dst, ss, rs, dev):
        return pltpu.make_async_remote_copy(
            src_ref=src, dst_ref=dst, send_sem=ss, recv_sem=rs, device_id=dev, device_id_type=MESH
        )

    h = x * (1 - t) + y * t
    near = rpeer[0] * (1 - t) + rpeer[1] * t
    chunk = hd // CHUNKS

    def rows_of(side, c):
        return pl.ds(pl.multiple_of(side * hd + c * chunk, chunk), chunk)

    cols = pl.ds(pl.multiple_of(t * hr, hr), hr)
    last = 3

    def line(p, c, way, s, arrive=False):
        rows = rows_of(h, c)
        step = -1 if way == 0 else 1
        slab = f + step * s + (step if arrive else 0)
        dst = gath.at[p, slab, rows, :]
        src = base.at[p, rows, cols] if s == 0 and not arrive else dst
        dev = f + step if arrive else f - step
        return remote(src, dst, az_s.at[p, c, way, s], az_r.at[p, c, way, s], (dev, r, t))

    def sends_line(way, s):
        return (f >= s) & (f < last) if way == 0 else (f + s <= last) & (f > 0)

    def gets_line(way, s):
        return f >= s + 1 if way == 0 else f + s + 1 <= last

    def share_slab(p, c, slab):
        rows = rows_of(h, c)
        return remote(
            gath.at[p, slab, rows, :], gath.at[p, slab, rows, :],
            aw_s.at[p, c, slab], aw_r.at[p, c, slab], (f, near, t),
        )

    def got_slab(p, c, slab):
        orow = rows_of(1 - h, c)
        return remote(
            gath.at[p, slab, orow, :], gath.at[p, slab, orow, :],
            aw_s.at[p, c, slab], aw_r.at[p, c, slab], (f, near, t),
        )

    def open_line(p):
        loads[p].wait()
        for c in range(CHUNKS):
            for way in range(2):
                @pl.when(sends_line(way, 0))
                def _():
                    line(p, c, way, 0).start()

    def run_line(s, p):
        for c in range(CHUNKS):
            for way in range(2):
                @pl.when(gets_line(way, s))
                def _():
                    line(p, c, way, s, True).wait_recv()
                    slab = f - 1 - s if way == 0 else f + 1 + s
                    share_slab(p, c, slab).start()
                if s < 2:
                    @pl.when(sends_line(way, s + 1))
                    def _():
                        line(p, c, way, s + 1).start()

    def slab_dot(p, g, weights):
        return jnp.dot(
            act[p, :, pl.ds(pl.multiple_of(g * depth, depth), depth)], weights,
            preferred_element_type=jnp.float32,
        )

    def project(p, acc):
        for g in fsrc:
            for c in range(CHUNKS):
                got_slab(p, c, g).wait_recv()
            acc = acc + slab_dot(p, g, gath[p, g])
        xb[p, t] = acc.astype(jnp.bfloat16)
        c = remote(xb.at[p, t], xb.at[p, t], xc_s.at[p], xc_r.at[p], (f, r, ot))
        c.start()
        return c

    def got_half(p):
        return remote(xb.at[p, ot], xb.at[p, ot], xc_s.at[p], xc_r.at[p], (f, r, ot))

    def scatter_reps(p):
        loads[4 + p].wait()
        got_half(p).wait_recv()
        for j in range(2):
            part = lax.dot_general(
                xb[p, j], cot[p], (((0,), (0,)), ((), ())), preferred_element_type=jnp.float32
            )
            for i in range(2):
                pb[p, 2 * j + i] = part[i * share : (i + 1) * share].astype(jnp.bfloat16)
        out = []
        for k in (2, 0, 1):
            c = remote(
                pb.at[p, rpeer[k]], t1.at[p, k], b1_s.at[p, k], b1_r.at[p, k], (f, rpeer[k], t)
            )
            c.start()
            out.append(c)
        return out

    piece = share // 4

    def scatter_tokens(p, arrivals):
        for c in arrivals:
            c.wait_recv()
        total = pb[p, r].astype(jnp.float32)
        for k in range(3):
            total = total + t1[p, k].astype(jnp.float32)
        for g in range(4):
            sb[p, g] = total[g * piece : (g + 1) * piece].astype(jnp.bfloat16)
        out = []
        for k in (2, 0, 1):
            c = remote(
                sb.at[p, fpeer[k]], t2.at[p, k], b2_s.at[p, k], b2_r.at[p, k], (fpeer[k], r, t)
            )
            c.start()
            out.append(c)
        return out

    def gather_sums(p, arrivals):
        for c in arrivals:
            c.wait_recv()
        total = sb[p, f].astype(jnp.float32)
        for k in range(3):
            total = total + t2[p, k].astype(jnp.float32)
        ag[p, f] = total.astype(jnp.bfloat16)
        out = []
        for k in (2, 0, 1):
            c = remote(
                ag.at[p, f], ag.at[p, f], g_s.at[p, k], g_r.at[p, k], (fpeer[k], r, t)
            )
            c.start()
            out.append(c)
        return out

    def got_sums(p, k):
        src = fsrc[k]
        return remote(ag.at[p, src], ag.at[p, src], g_s.at[p, k], g_r.at[p, k], (src, r, t))

    others = [(q, s) for q in rpeer for s in (t, ot)] + [(r, ot)]
    me = 2 * r + t

    def update_moment(p):
        old = mq[...] if p == 0 else mo[...].T
        for k in range(3):
            got_sums(p, k).wait_recv()
        total = ag[p].astype(jnp.float32).reshape(old.shape)
        new = BETA * old + (1.0 - BETA) * total
        mom[p] = new
        sq = new * new
        lanes = sq[:, :128]
        for k in range(1, sq.shape[1] // 128):
            lanes = lanes + sq[:, k * 128 : (k + 1) * 128]
        acc = lanes[:8]
        for k in range(1, share // 8):
            acc = acc + lanes[k * 8 : (k + 1) * 8]
        nrm[p, me] = acc
        out = []
        for k, (q, s) in enumerate(others):
            c = remote(nrm.at[p, me], nrm.at[p, me], n_s.at[p, k], n_r.at[p, k], (f, q, s))
            c.start()
            out.append(c)
        return out

    def gather_dirs(p):
        for k, (q, s) in enumerate(others):
            slot = 2 * q + s
            remote(
                nrm.at[p, slot], nrm.at[p, slot], n_s.at[p, k], n_r.at[p, k], (f, q, s)
            ).wait_recv()
        acc = nrm[p, 0]
        for k in range(1, 8):
            acc = acc + nrm[p, k]
        squares = jnp.sum(jnp.sum(acc, axis=0, keepdims=True), axis=1, keepdims=True)
        full[p, r] = (mom[p] * lax.rsqrt(squares / entries + EPS)).astype(jnp.bfloat16)
        out = []
        for k in (2, 0, 1):
            c = remote(
                full.at[p, r], full.at[p, r], d_s.at[p, k], d_r.at[p, k], (f, rpeer[k], t)
            )
            c.start()
            out.append(c)
        return out

    open_line(0)
    open_line(1)
    loads[2].wait()
    loads[3].wait()
    accs = [slab_dot(p, f, base[p, :, cols]) for p in range(2)]
    for s in range(3):
        run_line(s, 0)
        run_line(s, 1)
    x0 = project(0, accs[0])
    b1q = scatter_reps(0)
    x1 = project(1, accs[1])
    b2q = scatter_tokens(0, b1q)
    b1o = scatter_reps(1)
    gq = gather_sums(0, b2q)
    b2o = scatter_tokens(1, b1o)
    loads[6].wait()
    nq = update_moment(0)
    go = gather_sums(1, b2o)
    dq = gather_dirs(0)
    loads[7].wait()
    no = update_moment(1)
    stores = []
    for p in range(2):
        c = pltpu.make_async_copy(mom.at[p], mom_out.at[p], store_sem.at[p])
        c.start()
        stores.append(c)
    do = gather_dirs(1)
    for p in range(2):
        for k in range(3):
            remote(
                full.at[p, rpeer[k]], full.at[p, rpeer[k]],
                d_s.at[p, k], d_r.at[p, k], (f, rpeer[k], t),
            ).wait_recv()
        c = pltpu.make_async_copy(full.at[p], full_out.at[p], store_sem.at[2 + p])
        c.start()
        stores.append(c)
    for p in range(2):
        for c in range(CHUNKS):
            for s in range(3):
                for way in range(2):
                    @pl.when(sends_line(way, s))
                    def _():
                        line(p, c, way, s).wait_send()
            for g in fsrc:
                share_slab(p, c, g).wait_send()
    for group in (b1q, b1o, b2q, b2o, gq, go, nq, no, dq, do, [x0, x1]):
        for c in group:
            c.wait_send()
    for c in stores:
        c.wait()


def finish_kernel(
    qb, ob, fq, fo, qw, ow, mq, mo, qs_o, os_o, qn_o, on_o, qc_o, oc_o, mq_o, mo_o
):
    step = jnp.dot(qb[...], fq[0], preferred_element_type=jnp.float32)
    new = qw[...] - RATE * step
    qs_o[...] = step
    qn_o[...] = new
    qc_o[...] = new.astype(jnp.bfloat16)
    step = lax.dot_general(
        fo[0].T, ob[...], (((1,), (1,)), ((), ())), preferred_element_type=jnp.float32
    )
    new = ow[...] - RATE * step
    os_o[...] = step
    on_o[...] = new
    oc_o[...] = new.astype(jnp.bfloat16)
    mq_o[...] = mq[0]
    mo_o[...] = mo[0].T


def on_device_fast(
    saved_input, query_cot, attn_out, out_cot, query_basis, output_basis,
    query_weight, output_weight, query_moment, output_moment,
):
    tokens, depth_all = saved_input.shape
    width = query_cot.shape[1]
    depth, rank = query_basis.shape
    share = rank // 4
    entries = rank * width * lax.axis_size("tp")
    bf, f32 = jnp.bfloat16, jnp.float32
    any_spec = pl.BlockSpec(memory_space=pl.ANY)
    dma = pltpu.SemaphoreType.DMA
    full, mom = pl.pallas_call(
        functools.partial(exchange_kernel, entries),
        out_shape=(
            jax.ShapeDtypeStruct((2, 4, share, width), bf),
            jax.ShapeDtypeStruct((2, share, width), f32),
        ),
        in_specs=[any_spec] * 8,
        out_specs=(any_spec, any_spec),
        scratch_shapes=[
            pltpu.VMEM((2, tokens, depth_all), bf),
            pltpu.VMEM((2, tokens, width), bf),
            pltpu.VMEM((2, depth, rank), bf),
            pltpu.VMEM((share, width), f32),
            pltpu.VMEM((width, share), f32),
            pltpu.VMEM((2, 4, depth, rank // 2), bf),
            pltpu.VMEM((2, 2, tokens, rank // 2), bf),
            pltpu.VMEM((2, 4, share, width), bf),
            pltpu.VMEM((2, 3, share, width), bf),
            pltpu.VMEM((2, 4, share // 4, width), bf),
            pltpu.VMEM((2, 3, share // 4, width), bf),
            pltpu.VMEM((2, 4, share // 4, width), bf),
            pltpu.VMEM((2, share, width), f32),
            pltpu.VMEM((2, 8, 8, 128), f32),
            pltpu.VMEM((2, 4, share, width), bf),
            dma((8,)), dma((4,)),
            dma((2, CHUNKS, 2, 3)), dma((2, CHUNKS, 2, 3)),
            dma((2, CHUNKS, 4)), dma((2, CHUNKS, 4)),
            dma((2,)), dma((2,)),
            dma((2, 3)), dma((2, 3)), dma((2, 3)), dma((2, 3)), dma((2, 3)), dma((2, 3)),
            dma((2, 7)), dma((2, 7)), dma((2, 3)), dma((2, 3)),
        ],
        compiler_params=pltpu.CompilerParams(
            collective_id=0, has_side_effects=True, vmem_limit_bytes=60 * 2**20
        ),
    )(
        saved_input, out_cot, query_cot, attn_out, query_basis, output_basis,
        query_moment, output_moment,
    )
    full = full.reshape(2, rank, width)
    n = 4
    rows = pl.BlockSpec((depth // n, rank), lambda i: (i, 0))
    whole = pl.BlockSpec((depth, rank), lambda i: (0, 0))
    wq = pl.BlockSpec((depth // n, width), lambda i: (i, 0))
    wo = pl.BlockSpec((width // n, depth), lambda i: (i, 0))
    mq = pl.BlockSpec((share // n, width), lambda i: (i, 0))
    mo = pl.BlockSpec((width // n, share), lambda i: (i, 0))
    sq, so = query_weight.shape, output_weight.shape
    return pl.pallas_call(
        finish_kernel,
        grid=(n,),
        out_shape=tuple(
            jax.ShapeDtypeStruct(s, d)
            for s, d in (
                (sq, f32), (so, f32), (sq, f32), (so, f32), (sq, bf), (so, bf),
                (query_moment.shape, f32), (output_moment.shape, f32),
            )
        ),
        in_specs=[
            rows, whole,
            pl.BlockSpec((1, rank, width), lambda i: (0, 0, 0)),
            pl.BlockSpec((1, rank, width // n), lambda i: (1, 0, i)),
            wq, wo,
            pl.BlockSpec((1, share // n, width), lambda i: (0, i, 0)),
            pl.BlockSpec((1, share, width // n), lambda i: (1, 0, i)),
        ],
        out_specs=(wq, wo, wq, wo, wq, wo, mq, mo),
        cost_estimate=pl.CostEstimate(
            flops=4 * depth * rank * width, bytes_accessed=20 * depth * width, transcendentals=0
        ),
    )(query_basis, output_basis, full, full, query_weight, output_weight, mom, mom)


def solution(mesh):
    small = dict(mesh.shape) == {"fs": 4, "rep": 4, "tp": 2}
    body = on_device_fast if small else on_device
    placed = (
        P(("fs", "rep"), None),
        P(("fs", "rep"), "tp"),
        P(("fs", "rep"), "tp"),
        P(("fs", "rep"), None),
        P("fs", None),
        P("fs", None),
        P("fs", "tp"),
        P("tp", "fs"),
        P("rep", "tp"),
        P("tp", "rep"),
    )
    return jax.shard_map(
        body,
        mesh=mesh,
        in_specs=placed,
        out_specs=(
            P("fs", "tp"),
            P("tp", "fs"),
            P("fs", "tp"),
            P("tp", "fs"),
            P("fs", "tp"),
            P("tp", "fs"),
            P("rep", "tp"),
            P("tp", "rep"),
        ),
        check_vma=False,
    )
```

profile of v0, /device:TPU:0, one launch (start us, length us, event | category | flops | bytes accessed | tf_op | source)
XLA Modules:
  0.0 72.6 jit_solution(1953580606631652462)
XLA Ops:
  0.6 66.0 %shard_map.161 = (bf16[2,4,128,512]{3,2,1,0:T(8,128)(2,1)}, f32[2,128,512]{2,1,0:T(8,128)}) custom-call(bf16[352,2048]{1,0:T(8,128)(2,1)} %si_hbm.1, bf16[352,2048]{1,0:T(8,128)(2,1)} %oc_hbm.1, bf16[352,512]{1,0:T(8,128)(2,1)} %qc_hbm.1, bf16[352,512]{1,0:T(8,128)(2,1)} %ao_hbm.1, bf16[512,512]{1,0:T(8,128)(2,1)} %qb.1, bf16[512,512]{1,0:T(8,128)(2,1)} %ob.1, ...), custom_call_target="tpu_custom_call" | custom-call | tf_op jit(solution)/shard_map/pallas_call | solution.py:401
  66.6 6.0 %shard_map.162 = (f32[512,512]{1,0:T(8,128)}, f32[512,512]{1,0:T(8,128)}, f32[512,512]{1,0:T(8,128)}, f32[512,512]{1,0:T(8,128)}, bf16[512,512]{1,0:T(8,128)(2,1...) custom-call(bf16[512,512]{1,0:T(8,128)(2,1)} %qb.1, bf16[512,512]{1,0:T(8,128)(2,1)} %ob.1, ...), custom_call_target="tpu_custom_call" | custom-call | flops 536870912 | bytes 5242880 | tf_op jit(solution)/shard_map/pallas_call | solution.py:448
where the time goes:
time: 72.8 us; the launch traced here: 72.6 us
  Pallas kernels  72 us (99%)
    pallas_call x1, Pallas kernels, on_device_fast(): pl.pallas_call(functools.partial(exchange_kernel, entries), out_shape=(ja...  66 us
    pallas_call x1, Pallas kernels, on_device_fast(): pl.pallas_call(finish_kernel, grid=(n,), out_shape=tuple((jax.ShapeDtypeS...  5.97 us

commit v1 on v0

v1 whole, which is shorter than its diff:
```python
import functools

import jax
import jax.numpy as jnp
from jax import lax
from jax.experimental import pallas as pl
from jax.experimental.pallas import tpu as pltpu
from jax.sharding import PartitionSpec as P

BETA = 0.8
RATE = 0.2
EPS = 1e-06


def on_device(
    saved_input,
    query_cot,
    attn_out,
    out_cot,
    query_basis,
    output_basis,
    query_weight,
    output_weight,
    query_moment,
    output_moment,
):
    rank = query_basis.shape[1]
    grad_rows = lax.psum_scatter(
        jnp.dot(saved_input.T, query_cot, preferred_element_type=jnp.float32),
        "fs",
        scatter_dimension=0,
        tiled=True,
    )
    query_part = jnp.dot(
        query_basis.astype(jnp.float32).T, grad_rows, precision=lax.Precision.HIGHEST
    )
    cot_proj = jnp.dot(
        out_cot,
        lax.all_gather(output_basis, "fs", axis=0, tiled=True),
        preferred_element_type=jnp.float32,
    )
    output_part = jnp.dot(attn_out.astype(jnp.float32).T, cot_proj, precision=lax.Precision.HIGHEST)
    reps = lax.axis_size("rep")
    share = rank // reps
    query_terms, output_terms = (
        lax.all_to_all(
            query_part.astype(jnp.bfloat16), "rep", split_axis=0, concat_axis=0, tiled=True
        ).astype(query_part.dtype),
        lax.all_to_all(
            output_part.T.astype(jnp.bfloat16), "rep", split_axis=0, concat_axis=0, tiled=True
        ).astype(jnp.float32),
    )
    width = query_part.shape[1]
    query_local = jnp.sum(query_terms.reshape(reps, share, width), axis=0)
    output_local = jnp.sum(output_terms.reshape(reps, share, width), axis=0)
    query_share, output_flip = lax.psum((query_local, output_local), "fs")
    output_share = output_flip.T
    query_moment_new = BETA * query_moment + (1.0 - BETA) * query_share
    output_moment_new = BETA * output_moment + (1.0 - BETA) * output_share
    query_squares, output_squares = lax.psum(
        (
            jnp.sum(query_moment_new * query_moment_new),
            jnp.sum(output_moment_new * output_moment_new),
        ),
        ("rep", "tp"),
    )
    entries = rank * query_moment.shape[1] * lax.axis_size("tp")
    query_dir = (query_moment_new * lax.rsqrt(query_squares / entries + EPS)).astype(jnp.bfloat16)
    output_dir = (output_moment_new * lax.rsqrt(output_squares / entries + EPS)).astype(
        jnp.bfloat16
    )
    query_full, output_full = (
        lax.all_gather(query_dir, "rep", axis=0, tiled=True),
        lax.all_gather(output_dir, "rep", axis=1, tiled=True),
    )
    query_step = jnp.dot(query_basis, query_full, preferred_element_type=jnp.float32)
    output_step = jnp.dot(output_full, output_basis.T, preferred_element_type=jnp.float32)
    query_new = query_weight - RATE * query_step
    output_new = output_weight - RATE * output_step
    return (
        query_step,
        output_step,
        query_new,
        output_new,
        query_new.astype(jnp.bfloat16),
        output_new.astype(jnp.bfloat16),
        query_moment_new,
        output_moment_new,
    )


MESH = pl.DeviceIdType.MESH
UNITS = 4


def exchange_kernel(
    si_hbm, oc_hbm, qc_hbm, ao_hbm, qb_hbm, ob_hbm, mq_hbm, mo_hbm,
    full_out, mom_out, norm_out,
    act, cot, base, old, mo, gath, pb, t1, sb, t2, ag, mom, nrm, full, total_sq,
    load_sem, store_sem, cx_s, cx_r, az_s, az_r, aw_s, aw_r,
    b1_s, b1_r, b2_s, b2_r, g_s, g_r, n_s, n_r, d_s, d_r,
):
    f, r, t = lax.axis_index("fs"), lax.axis_index("rep"), lax.axis_index("tp")
    y, x = r // 2, r % 2
    ot = 1 - t
    fpeer = [(f + d) % 4 for d in (1, 3, 2)]
    fsrc = [(f + 4 - d) % 4 for d in (1, 3, 2)]
    rpeer = [2 * y + (1 - x), 2 * (1 - y) + x, 3 - r]
    depth, half = base.shape[1], base.shape[2]
    hd = depth // 2
    share = half // 2
    cut = share // 2
    piece = cut // 4

    cols = pl.ds(pl.multiple_of(t * half, half), half)
    loads = []
    for k, (src, dst) in enumerate((
        (qb_hbm.at[:, cols], base.at[0]), (ob_hbm.at[:, cols], base.at[1]),
        (qc_hbm, cot.at[0, t]), (ao_hbm, cot.at[1, t]),
        (si_hbm, act.at[0]), (oc_hbm, act.at[1]),
        (mq_hbm, old.at[0]), (mo_hbm, mo),
    )):
        c = pltpu.make_async_copy(src, dst, load_sem.at[k])
        c.start()
        loads.append(c)

    barrier = pltpu.get_barrier_semaphore()
    for g in fpeer:
        pl.semaphore_signal(barrier, inc=1, device_id=(g, r, t), device_id_type=MESH)
    for q in rpeer:
        for s in (t, ot):
            pl.semaphore_signal(barrier, inc=1, device_id=(f, q, s), device_id_type=MESH)
    pl.semaphore_signal(barrier, inc=1, device_id=(f, r, ot), device_id_type=MESH)

    for p in range(2):
        loads[p].wait()
        lo, hi = base[p, :, :share], base[p, :, share:]
        gath[2 * p, f] = jnp.concatenate([lo[:, :cut], hi[:, :cut]], axis=1)
        gath[2 * p + 1, f] = jnp.concatenate([lo[:, cut:], hi[:, cut:]], axis=1)

    pl.semaphore_wait(barrier, 10)

    def remote(src, dst, ss, rs, dev):
        return pltpu.make_async_remote_copy(
            src_ref=src, dst_ref=dst, send_sem=ss, recv_sem=rs, device_id=dev, device_id_type=MESH
        )

    h = x * (1 - t) + y * t
    near = rpeer[0] * (1 - t) + rpeer[1] * t
    mine = pl.ds(pl.multiple_of(h * hd, hd), hd)
    theirs = pl.ds(pl.multiple_of((1 - h) * hd, hd), hd)
    last = 3

    def line(u, way, s, arrive=False):
        step = -1 if way == 0 else 1
        slab = f + step * s + (step if arrive else 0)
        ref = gath.at[u, slab, mine, :]
        dev = f + step if arrive else f - step
        return remote(ref, ref, az_s.at[u, way, s], az_r.at[u, way, s], (dev, r, t))

    def sends_line(way, s):
        return (f >= s) & (f < last) if way == 0 else (f + s <= last) & (f > 0)

    def gets_line(way, s):
        return f >= s + 1 if way == 0 else f + s + 1 <= last

    def carried(way):
        return f if way == 0 else last - f

    def share_slab(u, slab, rows):
        ref = gath.at[u, slab, rows, :]
        return remote(ref, ref, aw_s.at[u, slab], aw_r.at[u, slab], (f, near, t))

    def open_line(u, count=None):
        for way in range(2):
            go = sends_line(way, 0)
            if count is not None:
                go = go & (carried(way) == count)

            @pl.when(go)
            def _():
                line(u, way, 0).start()

    def run_line(u, s):
        for way in range(2):
            @pl.when(gets_line(way, s))
            def _():
                line(u, way, s, True).wait_recv()
            if s < 2:
                @pl.when(sends_line(way, s + 1))
                def _():
                    line(u, way, s + 1).start()

            @pl.when(gets_line(way, s))
            def _():
                slab = f - 1 - s if way == 0 else f + 1 + s
                share_slab(u, slab, mine).start()

    def swap_cot(p):
        ref = cot.at[p, t]
        return remote(ref, ref, cx_s.at[p], cx_r.at[p], (f, r, ot))

    def got_cot(p):
        ref = cot.at[p, ot]
        return remote(ref, ref, cx_s.at[p], cx_r.at[p], (f, r, ot))

    def to_reps(u, k):
        j = 1 - x if k < 2 else x
        c = (0, 1, ot, t)[k]
        return remote(
            pb.at[u, j, c], t1.at[u, r], b1_s.at[u, k], b1_r.at[u, r], (f, 2 * t + j, c)
        )

    def from_rep(u, q):
        return remote(t1.at[u, q], t1.at[u, q], b1_s.at[u, 0], b1_r.at[u, q], (f, q, y))

    def scatter_reps(u):
        p = u // 2
        for g in fsrc:
            share_slab(u, g, theirs).wait_recv()
        part = jnp.dot(act[p, :, :depth], gath[u, 0], preferred_element_type=jnp.float32)
        for g in range(1, 4):
            part = part + jnp.dot(
                act[p, :, g * depth : (g + 1) * depth], gath[u, g],
                preferred_element_type=jnp.float32,
            )
        part = part.astype(jnp.bfloat16)
        for c in range(2):
            terms = lax.dot_general(
                part, cot[p, c], (((0,), (0,)), ((), ())), preferred_element_type=jnp.float32
            )
            for j in range(2):
                pb[u, j, c] = terms[j * cut : (j + 1) * cut].astype(jnp.bfloat16)
        for k in range(3):
            to_reps(u, k).start()

        @pl.when(t != y)
        def _():
            to_reps(u, 3).start()

        @pl.when(t == y)
        def _():
            t1[u, r] = pb[u, x, t]

    def scatter_tokens(u):
        for q in (rpeer[0], rpeer[1], rpeer[2]):
            from_rep(u, q).wait_recv()

        @pl.when(t != y)
        def _():
            from_rep(u, r).wait_recv()

        total = t1[u, 0].astype(jnp.float32)
        for q in range(1, 4):
            total = total + t1[u, q].astype(jnp.float32)
        for g in range(4):
            sb[u, g] = total[g * piece : (g + 1) * piece].astype(jnp.bfloat16)
        for k in (2, 0, 1):
            to_token(u, k).start()

    def to_token(u, k):
        return remote(
            sb.at[u, fpeer[k]], t2.at[u, k], b2_s.at[u, k], b2_r.at[u, k], (fpeer[k], r, t)
        )

    def rows_at(u, g):
        at = (u % 2) * cut + g * piece
        return pl.ds(pl.multiple_of(at, piece), piece)

    def to_dirs(u, g, k):
        ref = full.at[u // 2, r, rows_at(u, g), :]
        return remote(ref, ref, d_s.at[u, g, k], d_r.at[u, g, k], (f, rpeer[k], t))

    def got_dirs(u, g, k):
        ref = full.at[u // 2, rpeer[k], rows_at(u, g), :]
        return remote(ref, ref, d_s.at[u, g, k], d_r.at[u, g, k], (f, rpeer[k], t))

    def to_sums(u, k):
        return remote(
            ag.at[u, f], ag.at[u, f], g_s.at[u, k], g_r.at[u, k], (fpeer[k], r, t)
        )

    def got_sums(u, k):
        ref = ag.at[u, fsrc[k]]
        return remote(ref, ref, g_s.at[u, k], g_r.at[u, k], (fsrc[k], r, t))

    def update(u, g):
        p, rows = u // 2, rows_at(u, g)
        new = BETA * old[p, rows, :] + (1.0 - BETA) * ag[u, g].astype(jnp.float32)
        mom[p, rows, :] = new
        full[p, r, rows, :] = new.astype(jnp.bfloat16)
        for k in (2, 0, 1):
            to_dirs(u, g, k).start()

    def gather_sums(u):
        total = sb[u, f].astype(jnp.float32)
        for k in range(3):
            to_token(u, k).wait_recv()
            total = total + t2[u, k].astype(jnp.float32)
        ag[u, f] = total.astype(jnp.bfloat16)
        for k in (2, 0, 1):
            to_sums(u, k).start()
        update(u, f)

    def gather_dirs(u):
        for k in range(3):
            got_sums(u, k).wait_recv()
            update(u, fsrc[k])

    others = [(q, s) for q in rpeer for s in (t, ot)] + [(r, ot)]
    me = 2 * r + t

    def to_norms(p, k):
        q, s = others[k]
        ref = nrm.at[p, me]
        return remote(ref, ref, n_s.at[p, k], n_r.at[p, k], (f, q, s))

    def got_norms(p, k):
        q, s = others[k]
        ref = nrm.at[p, 2 * q + s]
        return remote(ref, ref, n_s.at[p, k], n_r.at[p, k], (f, q, s))

    def send_norms(p):
        sq = mom[p] * mom[p]
        lanes = sq[:, :128]
        for k in range(1, sq.shape[1] // 128):
            lanes = lanes + sq[:, k * 128 : (k + 1) * 128]
        acc = lanes[:8]
        for k in range(1, share // 8):
            acc = acc + lanes[k * 8 : (k + 1) * 8]
        nrm[p, me] = acc
        for k in range(7):
            to_norms(p, k).start()

    def sum_norms(p):
        for k in range(7):
            got_norms(p, k).wait_recv()
        acc = nrm[p, 0]
        for k in range(1, 8):
            acc = acc + nrm[p, k]
        total_sq[p] = acc

    def stores(p):
        return [
            pltpu.make_async_copy(full.at[p], full_out.at[p], store_sem.at[p, 0]),
            pltpu.make_async_copy(mom.at[p], mom_out.at[p], store_sem.at[p, 1]),
            pltpu.make_async_copy(total_sq.at[p], norm_out.at[p], store_sem.at[p, 2]),
        ]

    def finish(p):
        stores(p)[1].start()
        sum_norms(p)
        stores(p)[2].start()
        for u in (2 * p, 2 * p + 1):
            for g in [f] + fsrc:
                for k in range(3):
                    got_dirs(u, g, k).wait_recv()
        stores(p)[0].start()

    open_line(0)
    open_line(1)
    open_line(2, 0)
    open_line(3, 0)
    for p in range(2):
        loads[2 + p].wait()
        swap_cot(p).start()
    loads[6].wait()
    loads[7].wait()
    old[1] = mo[...].T
    run_line(0, 0)
    run_line(1, 0)
    open_line(2, 1)
    run_line(0, 1)
    run_line(1, 1)
    open_line(2, 2)
    run_line(2, 0)
    open_line(3, 1)
    run_line(0, 2)
    run_line(1, 2)
    loads[4].wait()
    got_cot(0).wait_recv()
    scatter_reps(0)
    run_line(2, 1)
    open_line(3, 2)
    scatter_reps(1)
    run_line(3, 0)
    run_line(2, 2)
    run_line(3, 1)
    loads[5].wait()
    got_cot(1).wait_recv()
    scatter_reps(2)
    run_line(3, 2)
    scatter_tokens(0)
    scatter_reps(3)
    scatter_tokens(1)
    gather_sums(0)
    scatter_tokens(2)
    gather_sums(1)
    scatter_tokens(3)
    gather_dirs(0)
    gather_sums(2)
    gather_dirs(1)
    send_norms(0)
    gather_sums(3)
    gather_dirs(2)
    gather_dirs(3)
    send_norms(1)
    finish(0)
    finish(1)
    for u in range(UNITS):
        for way in range(2):
            for s in range(3):
                @pl.when(sends_line(way, s))
                def _():
                    line(u, way, s).wait_send()
        for k in range(3):
            share_slab(u, fsrc[k], mine).wait_send()
            to_reps(u, k).wait_send()
            to_token(u, k).wait_send()
            to_sums(u, k).wait_send()
            for g in range(4):
                to_dirs(u, g, k).wait_send()

        @pl.when(t != y)
        def _():
            to_reps(u, 3).wait_send()

    for p in range(2):
        swap_cot(p).wait_send()
        for k in range(7):
            to_norms(p, k).wait_send()
        for c in stores(p):
            c.wait()


def finish_kernel(
    entries, qb, ob, fq, fo, sq, qw, ow, mq, mo,
    qs_o, os_o, qn_o, on_o, qc_o, oc_o, mq_o, mo_o,
):
    def scale(p):
        rows = jnp.sum(sq[p], axis=0, keepdims=True)
        return lax.rsqrt(jnp.sum(rows, axis=1, keepdims=True) / entries + EPS)

    step = jnp.dot(qb[...], fq[0], preferred_element_type=jnp.float32) * scale(0)
    new = qw[...] - RATE * step
    qs_o[...] = step
    qn_o[...] = new
    qc_o[...] = new.astype(jnp.bfloat16)
    step = lax.dot_general(
        fo[0].T, ob[...], (((1,), (1,)), ((), ())), preferred_element_type=jnp.float32
    ) * scale(1)
    new = ow[...] - RATE * step
    os_o[...] = step
    on_o[...] = new
    oc_o[...] = new.astype(jnp.bfloat16)
    mq_o[...] = mq[0]
    mo_o[...] = mo[0].T


def on_device_fast(
    saved_input, query_cot, attn_out, out_cot, query_basis, output_basis,
    query_weight, output_weight, query_moment, output_moment,
):
    tokens, depth_all = saved_input.shape
    width = query_cot.shape[1]
    depth, rank = query_basis.shape
    share = rank // 4
    cut = share // 2
    piece = cut // 4
    entries = rank * width * lax.axis_size("tp")
    bf, f32 = jnp.bfloat16, jnp.float32
    any_spec = pl.BlockSpec(memory_space=pl.ANY)
    dma = pltpu.SemaphoreType.DMA
    ins = (
        saved_input, out_cot, query_cot, attn_out, query_basis, output_basis,
        query_moment, output_moment,
    )
    full, mom, norm = pl.pallas_call(
        exchange_kernel,
        out_shape=(
            jax.ShapeDtypeStruct((2, 4, share, width), bf),
            jax.ShapeDtypeStruct((2, share, width), f32),
            jax.ShapeDtypeStruct((2, 8, 128), f32),
        ),
        in_specs=[any_spec] * 8,
        out_specs=(any_spec, any_spec, any_spec),
        scratch_shapes=[
            pltpu.VMEM((2, tokens, depth_all), bf),
            pltpu.VMEM((2, 2, tokens, width), bf),
            pltpu.VMEM((2, depth, rank // 2), bf),
            pltpu.VMEM((2, share, width), f32),
            pltpu.VMEM((width, share), f32),
            pltpu.VMEM((UNITS, 4, depth, share), bf),
            pltpu.VMEM((UNITS, 2, 2, cut, width), bf),
            pltpu.VMEM((UNITS, 4, cut, width), bf),
            pltpu.VMEM((UNITS, 4, piece, width), bf),
            pltpu.VMEM((UNITS, 3, piece, width), bf),
            pltpu.VMEM((UNITS, 4, piece, width), bf),
            pltpu.VMEM((2, share, width), f32),
            pltpu.VMEM((2, 8, 8, 128), f32),
            pltpu.VMEM((2, 4, share, width), bf),
            pltpu.VMEM((2, 8, 128), f32),
            dma((8,)), dma((2, 3)), dma((2,)), dma((2,)),
            dma((UNITS, 2, 3)), dma((UNITS, 2, 3)), dma((UNITS, 4)), dma((UNITS, 4)),
            dma((UNITS, 4)), dma((UNITS, 4)), dma((UNITS, 3)), dma((UNITS, 3)),
            dma((UNITS, 3)), dma((UNITS, 3)), dma((2, 7)), dma((2, 7)),
            dma((UNITS, 4, 3)), dma((UNITS, 4, 3)),
        ],
        compiler_params=pltpu.CompilerParams(
            collective_id=0, has_side_effects=True, vmem_limit_bytes=20 * 2**20
        ),
    )(*(pltpu.with_memory_space_constraint(a, pltpu.HBM) for a in ins))
    full = full.reshape(2, rank, width)
    n = 4
    rows = pl.BlockSpec((depth // n, rank), lambda i: (i, 0))
    whole = pl.BlockSpec((depth, rank), lambda i: (0, 0))
    wq = pl.BlockSpec((depth // n, width), lambda i: (i, 0))
    wo = pl.BlockSpec((width // n, depth), lambda i: (i, 0))
    mq = pl.BlockSpec((share // n, width), lambda i: (i, 0))
    mo = pl.BlockSpec((width // n, share), lambda i: (i, 0))
    sq, so = query_weight.shape, output_weight.shape
    return pl.pallas_call(
        functools.partial(finish_kernel, entries),
        grid=(n,),
        out_shape=tuple(
            jax.ShapeDtypeStruct(s, d)
            for s, d in (
                (sq, f32), (so, f32), (sq, f32), (so, f32), (sq, bf), (so, bf),
                (query_moment.shape, f32), (output_moment.shape, f32),
            )
        ),
        in_specs=[
            rows, whole,
            pl.BlockSpec((1, rank, width), lambda i: (0, 0, 0)),
            pl.BlockSpec((1, rank, width // n), lambda i: (1, 0, i)),
            pl.BlockSpec((2, 8, 128), lambda i: (0, 0, 0)),
            wq, wo,
            pl.BlockSpec((1, share // n, width), lambda i: (0, i, 0)),
            pl.BlockSpec((1, share, width // n), lambda i: (1, 0, i)),
        ],
        out_specs=(wq, wo, wq, wo, wq, wo, mq, mo),
        cost_estimate=pl.CostEstimate(
            flops=4 * depth * rank * width, bytes_accessed=20 * depth * width, transcendentals=0
        ),
        compiler_params=pltpu.CompilerParams(vmem_limit_bytes=20 * 2**20),
    )(query_basis, output_basis, full, full, norm, query_weight, output_weight, mom, mom)


def solution(mesh):
    small = dict(mesh.shape) == {"fs": 4, "rep": 4, "tp": 2}
    body = on_device_fast if small else on_device
    placed = (
        P(("fs", "rep"), None),
        P(("fs", "rep"), "tp"),
        P(("fs", "rep"), "tp"),
        P(("fs", "rep"), None),
        P("fs", None),
        P("fs", None),
        P("fs", "tp"),
        P("tp", "fs"),
        P("rep", "tp"),
        P("tp", "rep"),
    )
    return jax.shard_map(
        body,
        mesh=mesh,
        in_specs=placed,
        out_specs=(
            P("fs", "tp"),
            P("tp", "fs"),
            P("fs", "tp"),
            P("tp", "fs"),
            P("fs", "tp"),
            P("tp", "fs"),
            P("rep", "tp"),
            P("tp", "rep"),
        ),
        check_vma=False,
    )
```

time: 72.8 us -> 70 us (0.962)
  Pallas kernels: 72 us -> 69.1 us
    pallas_call x2, Pallas kernels: 72 us -> 69.1 us  [the longest x1 65.7 us: on_device_fast(): pl.pallas_call(exchange_kernel, out_shape=(jax.ShapeDtypeStruct((2, 4, sh...]
where the time goes in v1:
time: 70 us; the launch traced here: 69.8 us
  Pallas kernels  69.1 us (99%)
  between operations  0.71 us (1%)
    pallas_call x1, Pallas kernels, on_device_fast(): pl.pallas_call(exchange_kernel, out_shape=(jax.ShapeDtypeStruct((2, 4, sh...  65.7 us
    pallas_call x1, Pallas kernels, on_device_fast(): pl.pallas_call(functools.partial(finish_kernel, entries), grid=(n,), out_...  3.4 us

profile of v1, /device:TPU:0, one launch (start us, length us, event | category | flops | bytes accessed | tf_op | source)
XLA Modules:
  0.0 69.8 jit_solution(3903148270181518016)
XLA Ops:
  0.6 0.0 copy-start.1
  0.6 0.0 copy-start
  0.7 0.0 copy-start.3
  0.7 0.0 copy-start.2
  0.7 65.7 %shard_map.161 = (bf16[2,4,128,512]{3,2,1,0:T(8,128)(2,1)S(1)}, f32[2,128,512]{2,1,0:T(8,128)S(1)}, f32[2,8,128]{2,1,0:T(8,128)S(1)}) custom-call(bf16[352,2048]{1,0:T(8,128)(2,1)} %si_hbm.1, bf16[352,2048]{1,0:T(8,128)(2,1)} %oc_hbm.1, bf16[352,512]{1,0:T(8,128)(2,1)} %qc_hbm.1, bf16[352,512]{1,0:T(8,128)(2,1)} %ao_hbm.1, bf16[512,512]{1,0:T(8,128)(2,1)} %qb.1, ...), custom_call_target="tpu_custom_call" | custom-call | tf_op jit(solution)/shard_map/pallas_call | solution.py:478
  66.4 0.0 copy-done.1
  66.4 0.0 copy-done
  66.4 0.0 copy-done.3
  66.4 0.0 copy-done.2
  66.4 3.4 %shard_map.162 = (f32[512,512]{1,0:T(8,128)}, f32[512,512]{1,0:T(8,128)}, f32[512,512]{1,0:T(8,128)}, f32[512,512]{1,0:T(8,128)}, bf16[512,512]{1,0:T(8,128)(2,1...) custom-call(bf16[512,512]{1,0:T(8,128)(2,1)S(1)} %copy-done, bf16[512,512]{1,0:T(8,128)(2,1)S(1)} %copy-done.1, ...), custom_call_target="tpu_custom_call" | custom-call | flops 536870912 | bytes 5242880 | tf_op jit(solution)/shard_map/pallas_call | solution.py:522
Async XLA Ops:
  0.6 65.7 %copy-start.1 = (bf16[512,512]{1,0:T(8,128)(2,1)S(1)}, bf16[512,512]{1,0:T(8,128)(2,1)}, u32[]{:S(2)}) copy-start(bf16[512,512]{1,0:T(8,128)(2,1)} %ob.1) | copy-start | bytes 1572868
  0.6 65.7 %copy-start = (bf16[512,512]{1,0:T(8,128)(2,1)S(1)}, bf16[512,512]{1,0:T(8,128)(2,1)}, u32[]{:S(2)}) copy-start(bf16[512,512]{1,0:T(8,128)(2,1)} %qb.1) | copy-start | bytes 1572868
  0.7 65.7 %copy-start.3 = (f32[512,512]{1,0:T(8,128)S(1)}, f32[512,512]{1,0:T(8,128)}, u32[]{:S(2)}) copy-start(f32[512,512]{1,0:T(8,128)} %ow.1) | copy-start | bytes 3145732
  0.7 65.7 %copy-start.2 = (f32[512,512]{1,0:T(8,128)S(1)}, f32[512,512]{1,0:T(8,128)}, u32[]{:S(2)}) copy-start(f32[512,512]{1,0:T(8,128)} %qw.1) | copy-start | bytes 3145732

commit v2 on v1

--- a/solution.py
+++ b/solution.py
@@ -95,10 +95,9 @@
 
 def exchange_kernel(
     si_hbm, oc_hbm, qc_hbm, ao_hbm, qb_hbm, ob_hbm, mq_hbm, mo_hbm,
-    full_out, mom_out, norm_out,
-    act, cot, base, old, mo, gath, pb, t1, sb, t2, ag, mom, nrm, full, total_sq,
-    load_sem, store_sem, cx_s, cx_r, az_s, az_r, aw_s, aw_r,
-    b1_s, b1_r, b2_s, b2_r, g_s, g_r, n_s, n_r, d_s, d_r,
+    full, mom, total_sq,
+    act, cot, base, old, mo, gath, own, pb, t1, sb, t2, ag, nrm,
+    load_sem, sent, cx_r, az_r, aw_r, b1_r, b2_r, g_r, n_r, d_r,
 ):
     f, r, t = lax.axis_index("fs"), lax.axis_index("rep"), lax.axis_index("tp")
     y, x = r // 2, r % 2
@@ -135,8 +134,8 @@
     for p in range(2):
         loads[p].wait()
         lo, hi = base[p, :, :share], base[p, :, share:]
-        gath[2 * p, f] = jnp.concatenate([lo[:, :cut], hi[:, :cut]], axis=1)
-        gath[2 * p + 1, f] = jnp.concatenate([lo[:, cut:], hi[:, cut:]], axis=1)
+        gath[p, f, :, :share] = jnp.concatenate([lo[:, :cut], hi[:, :cut]], axis=1)
+        gath[p, f, :, share:] = jnp.concatenate([lo[:, cut:], hi[:, cut:]], axis=1)
 
     pl.semaphore_wait(barrier, 10)
 
@@ -144,6 +143,9 @@
         return pltpu.make_async_remote_copy(
             src_ref=src, dst_ref=dst, send_sem=ss, recv_sem=rs, device_id=dev, device_id_type=MESH
         )
+
+    def settle(ref, sem):
+        pltpu.make_async_copy(ref, ref, sem).wait()
 
     h = x * (1 - t) + y * t
     near = rpeer[0] * (1 - t) + rpeer[1] * t
@@ -151,12 +153,18 @@
     theirs = pl.ds(pl.multiple_of((1 - h) * hd, hd), hd)
     last = 3
 
+    def unit_ref(u, slab, rows):
+        k = u % 2
+        return gath.at[u // 2, slab, rows, k * share : (k + 1) * share]
+
     def line(u, way, s, arrive=False):
         step = -1 if way == 0 else 1
         slab = f + step * s + (step if arrive else 0)
-        ref = gath.at[u, slab, mine, :]
+        ref = unit_ref(u, slab, mine)
         dev = f + step if arrive else f - step
-        return remote(ref, ref, az_s.at[u, way, s], az_r.at[u, way, s], (dev, r, t))
+        to = f if arrive else dev
+        slot = s if way == 0 else to + s
+        return remote(ref, ref, sent.at[min(s, 1)], az_r.at[u, slot], (dev, r, t))
 
     def sends_line(way, s):
         return (f >= s) & (f < last) if way == 0 else (f + s <= last) & (f > 0)
@@ -168,8 +176,8 @@
         return f if way == 0 else last - f
 
     def share_slab(u, slab, rows):
-        ref = gath.at[u, slab, rows, :]
-        return remote(ref, ref, aw_s.at[u, slab], aw_r.at[u, slab], (f, near, t))
+        ref = unit_ref(u, slab, rows)
+        return remote(ref, ref, sent.at[2], aw_r.at[u], (f, near, t))
 
     def open_line(u, count=None):
         for way in range(2):
@@ -198,39 +206,38 @@
 
     def swap_cot(p):
         ref = cot.at[p, t]
-        return remote(ref, ref, cx_s.at[p], cx_r.at[p], (f, r, ot))
-
-    def got_cot(p):
-        ref = cot.at[p, ot]
-        return remote(ref, ref, cx_s.at[p], cx_r.at[p], (f, r, ot))
+        return remote(ref, ref, sent.at[3], cx_r.at[p], (f, r, ot))
 
     def to_reps(u, k):
         j = 1 - x if k < 2 else x
         c = (0, 1, ot, t)[k]
         return remote(
-            pb.at[u, j, c], t1.at[u, r], b1_s.at[u, k], b1_r.at[u, r], (f, 2 * t + j, c)
+            pb.at[u, j, c], t1.at[u, r], sent.at[4], b1_r.at[u], (f, 2 * t + j, c)
         )
 
-    def from_rep(u, q):
-        return remote(t1.at[u, q], t1.at[u, q], b1_s.at[u, 0], b1_r.at[u, q], (f, q, y))
-
-    def scatter_reps(u):
-        p = u // 2
+    def slab_dot(p, g, lanes):
+        at = pl.ds(pl.multiple_of(g * depth, depth), depth)
+        return jnp.dot(act[p, :, at], gath[p, g, :, lanes], preferred_element_type=jnp.float32)
+
+    def project(p, us):
+        for u in us:
+            k = u % 2
+            settle(gath.at[p, :3, theirs, k * share : (k + 1) * share], aw_r.at[u])
+        lanes = slice((us[0] % 2) * share, (us[-1] % 2 + 1) * share)
+        part = own[p, :, lanes]
         for g in fsrc:
-            share_slab(u, g, theirs).wait_recv()
-        part = jnp.dot(act[p, :, :depth], gath[u, 0], preferred_element_type=jnp.float32)
-        for g in range(1, 4):
-            part = part + jnp.dot(
-                act[p, :, g * depth : (g + 1) * depth], gath[u, g],
-                preferred_element_type=jnp.float32,
-            )
+            part = part + slab_dot(p, g, lanes)
         part = part.astype(jnp.bfloat16)
         for c in range(2):
             terms = lax.dot_general(
                 part, cot[p, c], (((0,), (0,)), ((), ())), preferred_element_type=jnp.float32
             )
-            for j in range(2):
-                pb[u, j, c] = terms[j * cut : (j + 1) * cut].astype(jnp.bfloat16)
+            for i, u in enumerate(us):
+                for j in range(2):
+                    at = i * share + j * cut
+                    pb[u, j, c] = terms[at : at + cut].astype(jnp.bfloat16)
+
+    def scatter_reps(u):
         for k in range(3):
             to_reps(u, k).start()
 
@@ -243,12 +250,13 @@
             t1[u, r] = pb[u, x, t]
 
     def scatter_tokens(u):
-        for q in (rpeer[0], rpeer[1], rpeer[2]):
-            from_rep(u, q).wait_recv()
-
         @pl.when(t != y)
         def _():
-            from_rep(u, r).wait_recv()
+            settle(t1.at[u], b1_r.at[u])
+
+        @pl.when(t == y)
+        def _():
+            settle(t1.at[u, :3], b1_r.at[u])
 
         total = t1[u, 0].astype(jnp.float32)
         for q in range(1, 4):
@@ -260,7 +268,7 @@
 
     def to_token(u, k):
         return remote(
-            sb.at[u, fpeer[k]], t2.at[u, k], b2_s.at[u, k], b2_r.at[u, k], (fpeer[k], r, t)
+            sb.at[u, fpeer[k]], t2.at[u, k], sent.at[5], b2_r.at[u], (fpeer[k], r, t)
         )
 
     def rows_at(u, g):
@@ -269,20 +277,12 @@
 
     def to_dirs(u, g, k):
         ref = full.at[u // 2, r, rows_at(u, g), :]
-        return remote(ref, ref, d_s.at[u, g, k], d_r.at[u, g, k], (f, rpeer[k], t))
-
-    def got_dirs(u, g, k):
-        ref = full.at[u // 2, rpeer[k], rows_at(u, g), :]
-        return remote(ref, ref, d_s.at[u, g, k], d_r.at[u, g, k], (f, rpeer[k], t))
+        return remote(ref, ref, sent.at[7], d_r.at[u // 2], (f, rpeer[k], t))
 
     def to_sums(u, k):
         return remote(
-            ag.at[u, f], ag.at[u, f], g_s.at[u, k], g_r.at[u, k], (fpeer[k], r, t)
+            ag.at[u, f], ag.at[u, f], sent.at[6], g_r.at[u, k], (fpeer[k], r, t)
         )
-
-    def got_sums(u, k):
-        ref = ag.at[u, fsrc[k]]
-        return remote(ref, ref, g_s.at[u, k], g_r.at[u, k], (fsrc[k], r, t))
 
     def update(u, g):
         p, rows = u // 2, rows_at(u, g)
@@ -294,8 +294,8 @@
 
     def gather_sums(u):
         total = sb[u, f].astype(jnp.float32)
+        settle(t2.at[u], b2_r.at[u])
         for k in range(3):
-            to_token(u, k).wait_recv()
             total = total + t2[u, k].astype(jnp.float32)
         ag[u, f] = total.astype(jnp.bfloat16)
         for k in (2, 0, 1):
@@ -304,7 +304,7 @@
 
     def gather_dirs(u):
         for k in range(3):
-            got_sums(u, k).wait_recv()
+            settle(ag.at[u, fsrc[k]], g_r.at[u, k])
             update(u, fsrc[k])
 
     others = [(q, s) for q in rpeer for s in (t, ot)] + [(r, ot)]
@@ -313,12 +313,7 @@
     def to_norms(p, k):
         q, s = others[k]
         ref = nrm.at[p, me]
-        return remote(ref, ref, n_s.at[p, k], n_r.at[p, k], (f, q, s))
-
-    def got_norms(p, k):
-        q, s = others[k]
-        ref = nrm.at[p, 2 * q + s]
-        return remote(ref, ref, n_s.at[p, k], n_r.at[p, k], (f, q, s))
+        return remote(ref, ref, sent.at[8], n_r.at[p], (f, q, s))
 
     def send_norms(p):
         sq = mom[p] * mom[p]
@@ -333,29 +328,15 @@
             to_norms(p, k).start()
 
     def sum_norms(p):
-        for k in range(7):
-            got_norms(p, k).wait_recv()
+        settle(nrm.at[p, :7], n_r.at[p])
         acc = nrm[p, 0]
         for k in range(1, 8):
             acc = acc + nrm[p, k]
         total_sq[p] = acc
 
-    def stores(p):
-        return [
-            pltpu.make_async_copy(full.at[p], full_out.at[p], store_sem.at[p, 0]),
-            pltpu.make_async_copy(mom.at[p], mom_out.at[p], store_sem.at[p, 1]),
-            pltpu.make_async_copy(total_sq.at[p], norm_out.at[p], store_sem.at[p, 2]),
-        ]
-
     def finish(p):
-        stores(p)[1].start()
         sum_norms(p)
-        stores(p)[2].start()
-        for u in (2 * p, 2 * p + 1):
-            for g in [f] + fsrc:
-                for k in range(3):
-                    got_dirs(u, g, k).wait_recv()
-        stores(p)[0].start()
+        settle(full.at[p, :3], d_r.at[p])
 
     open_line(0)
     open_line(1)
@@ -367,32 +348,35 @@
     loads[6].wait()
     loads[7].wait()
     old[1] = mo[...].T
+    for p in range(2):
+        loads[4 + p].wait()
+        own[p] = slab_dot(p, f, slice(None))
+        settle(cot.at[p, ot], cx_r.at[p])
     run_line(0, 0)
     run_line(1, 0)
     open_line(2, 1)
     run_line(0, 1)
     run_line(1, 1)
     open_line(2, 2)
+    run_line(0, 2)
+    run_line(1, 2)
     run_line(2, 0)
     open_line(3, 1)
-    run_line(0, 2)
-    run_line(1, 2)
-    loads[4].wait()
-    got_cot(0).wait_recv()
-    scatter_reps(0)
     run_line(2, 1)
     open_line(3, 2)
+    project(0, (0, 1))
+    run_line(2, 2)
+    scatter_reps(0)
     scatter_reps(1)
     run_line(3, 0)
-    run_line(2, 2)
+    project(1, (2,))
     run_line(3, 1)
-    loads[5].wait()
-    got_cot(1).wait_recv()
+    run_line(3, 2)
     scatter_reps(2)
-    run_line(3, 2)
     scatter_tokens(0)
+    scatter_tokens(1)
+    project(1, (3,))
     scatter_reps(3)
-    scatter_tokens(1)
     gather_sums(0)
     scatter_tokens(2)
     gather_sums(1)
@@ -407,30 +391,32 @@
     send_norms(1)
     finish(0)
     finish(1)
-    for u in range(UNITS):
-        for way in range(2):
-            for s in range(3):
-                @pl.when(sends_line(way, s))
-                def _():
-                    line(u, way, s).wait_send()
-        for k in range(3):
-            share_slab(u, fsrc[k], mine).wait_send()
-            to_reps(u, k).wait_send()
-            to_token(u, k).wait_send()
-            to_sums(u, k).wait_send()
-            for g in range(4):
-                to_dirs(u, g, k).wait_send()
-
-        @pl.when(t != y)
-        def _():
-            to_reps(u, 3).wait_send()
-
-    for p in range(2):
-        swap_cot(p).wait_send()
-        for k in range(7):
-            to_norms(p, k).wait_send()
-        for c in stores(p):
-            c.wait()
+    inner = (f > 0) & (f < last)
+
+    @pl.when(inner)
+    def _():
+        settle(gath.at[0, :2], sent.at[0])
+        settle(gath.at[0, :3], sent.at[1])
+
+    @pl.when(jnp.logical_not(inner))
+    def _():
+        settle(gath.at[0, :1], sent.at[0])
+
+    settle(gath.at[0, :3], sent.at[2])
+    settle(cot.at[0], sent.at[3])
+
+    @pl.when(t != y)
+    def _():
+        settle(pb, sent.at[4])
+
+    @pl.when(t == y)
+    def _():
+        settle(pb.at[:3], sent.at[4])
+
+    settle(t2, sent.at[5])
+    settle(t2, sent.at[6])
+    settle(full.at[:, :3], sent.at[7])
+    settle(nrm.at[:, :7], sent.at[8])
 
 
 def finish_kernel(
@@ -483,28 +469,23 @@
             jax.ShapeDtypeStruct((2, 8, 128), f32),
         ),
         in_specs=[any_spec] * 8,
-        out_specs=(any_spec, any_spec, any_spec),
+        out_specs=(pl.BlockSpec(memory_space=pltpu.VMEM),) * 3,
         scratch_shapes=[
             pltpu.VMEM((2, tokens, depth_all), bf),
             pltpu.VMEM((2, 2, tokens, width), bf),
             pltpu.VMEM((2, depth, rank // 2), bf),
             pltpu.VMEM((2, share, width), f32),
             pltpu.VMEM((width, share), f32),
-            pltpu.VMEM((UNITS, 4, depth, share), bf),
+            pltpu.VMEM((2, 4, depth, 2 * share), bf),
+            pltpu.VMEM((2, tokens, 2 * share), f32),
             pltpu.VMEM((UNITS, 2, 2, cut, width), bf),
             pltpu.VMEM((UNITS, 4, cut, width), bf),
             pltpu.VMEM((UNITS, 4, piece, width), bf),
             pltpu.VMEM((UNITS, 3, piece, width), bf),
             pltpu.VMEM((UNITS, 4, piece, width), bf),
-            pltpu.VMEM((2, share, width), f32),
             pltpu.VMEM((2, 8, 8, 128), f32),
-            pltpu.VMEM((2, 4, share, width), bf),
-            pltpu.VMEM((2, 8, 128), f32),
-            dma((8,)), dma((2, 3)), dma((2,)), dma((2,)),
-            dma((UNITS, 2, 3)), dma((UNITS, 2, 3)), dma((UNITS, 4)), dma((UNITS, 4)),
-            dma((UNITS, 4)), dma((UNITS, 4)), dma((UNITS, 3)), dma((UNITS, 3)),
-            dma((UNITS, 3)), dma((UNITS, 3)), dma((2, 7)), dma((2, 7)),
-            dma((UNITS, 4, 3)), dma((UNITS, 4, 3)),
+            dma((8,)), dma((9,)), dma((2,)), dma((UNITS, 3)), dma((UNITS,)), dma((UNITS,)),
+            dma((UNITS,)), dma((UNITS, 3)), dma((2,)), dma((2,)),
         ],
         compiler_params=pltpu.CompilerParams(
             collective_id=0, has_side_effects=True, vmem_limit_bytes=20 * 2**20

time: 70 us -> 56.7 us (0.81)
  Pallas kernels: 69.1 us -> 55.8 us
    pallas_call x1, Pallas kernels: 65.7 us -> 52.4 us  [on_device_fast(): pl.pallas_call(exchange_kernel, out_shape=(jax.ShapeDtypeStruct((2, 4, sh...]
where the time goes in v2:
time: 56.7 us; the launch traced here: 56.6 us
  Pallas kernels  55.8 us (98%)
  between operations  0.71 us (1%)
    pallas_call x1, Pallas kernels, on_device_fast(): pl.pallas_call(exchange_kernel, out_shape=(jax.ShapeDtypeStruct((2, 4, sh...  52.4 us
    pallas_call x1, Pallas kernels, on_device_fast(): pl.pallas_call(functools.partial(finish_kernel, entries), grid=(n,), out_...  3.4 us

profile of v2, /device:TPU:0, one launch (start us, length us, event | category | flops | bytes accessed | tf_op | source)
XLA Modules:
  0.0 56.6 jit_solution(608131530193612933)
XLA Ops:
  0.6 0.0 copy-start.1
  0.6 0.0 copy-start
  0.7 0.0 copy-start.3
  0.7 0.0 copy-start.2
  0.7 52.4 %shard_map.161 = (bf16[2,4,128,512]{3,2,1,0:T(8,128)(2,1)S(1)}, f32[2,128,512]{2,1,0:T(8,128)S(1)}, f32[2,8,128]{2,1,0:T(8,128)S(1)}) custom-call(bf16[352,2048]{1,0:T(8,128)(2,1)} %si_hbm.1, bf16[352,2048]{1,0:T(8,128)(2,1)} %oc_hbm.1, bf16[352,512]{1,0:T(8,128)(2,1)} %qc_hbm.1, bf16[352,512]{1,0:T(8,128)(2,1)} %ao_hbm.1, bf16[512,512]{1,0:T(8,128)(2,1)} %qb.1, ...), custom_call_target="tpu_custom_call" | custom-call | tf_op jit(solution)/shard_map/pallas_call | solution.py:464
  53.1 0.0 copy-done.1
  53.1 0.0 copy-done
  53.2 0.0 copy-done.3
  53.2 0.0 copy-done.2
  53.2 3.4 %shard_map.162 = (f32[512,512]{1,0:T(8,128)}, f32[512,512]{1,0:T(8,128)}, f32[512,512]{1,0:T(8,128)}, f32[512,512]{1,0:T(8,128)}, bf16[512,512]{1,0:T(8,128)(2,1...) custom-call(bf16[512,512]{1,0:T(8,128)(2,1)S(1)} %copy-done, bf16[512,512]{1,0:T(8,128)(2,1)S(1)} %copy-done.1, ...), custom_call_target="tpu_custom_call" | custom-call | flops 536870912 | bytes 5242880 | tf_op jit(solution)/shard_map/pallas_call | solution.py:503
Async XLA Ops:
  0.6 52.5 %copy-start.1 = (bf16[512,512]{1,0:T(8,128)(2,1)S(1)}, bf16[512,512]{1,0:T(8,128)(2,1)}, u32[]{:S(2)}) copy-start(bf16[512,512]{1,0:T(8,128)(2,1)} %ob.1) | copy-start | bytes 1572868
  0.6 52.5 %copy-start = (bf16[512,512]{1,0:T(8,128)(2,1)S(1)}, bf16[512,512]{1,0:T(8,128)(2,1)}, u32[]{:S(2)}) copy-start(bf16[512,512]{1,0:T(8,128)(2,1)} %qb.1) | copy-start | bytes 1572868
  0.7 52.5 %copy-start.3 = (f32[512,512]{1,0:T(8,128)S(1)}, f32[512,512]{1,0:T(8,128)}, u32[]{:S(2)}) copy-start(f32[512,512]{1,0:T(8,128)} %ow.1) | copy-start | bytes 3145732
  0.7 52.5 %copy-start.2 = (f32[512,512]{1,0:T(8,128)S(1)}, f32[512,512]{1,0:T(8,128)}, u32[]{:S(2)}) copy-start(f32[512,512]{1,0:T(8,128)} %qw.1) | copy-start | bytes 3145732

commit v3 on v2

--- a/solution.py
+++ b/solution.py
@@ -96,8 +96,8 @@
 def exchange_kernel(
     si_hbm, oc_hbm, qc_hbm, ao_hbm, qb_hbm, ob_hbm, mq_hbm, mo_hbm,
     full, mom, total_sq,
-    act, cot, base, old, mo, gath, own, pb, t1, sb, t2, ag, nrm,
-    load_sem, sent, cx_r, az_r, aw_r, b1_r, b2_r, g_r, n_r, d_r,
+    act, cot, head, base, old, mo, gath, own, pb, t1, sb, t2, ag, nrm, zb, zt, yb, yt,
+    load_sem, sent, cx_r, az_r, aw_r, b1_r, b2_r, g_r, n_r, d_r, z_r,
 ):
     f, r, t = lax.axis_index("fs"), lax.axis_index("rep"), lax.axis_index("tp")
     y, x = r // 2, r % 2
@@ -107,14 +107,16 @@
     rpeer = [2 * y + (1 - x), 2 * (1 - y) + x, 3 - r]
     depth, half = base.shape[1], base.shape[2]
     hd = depth // 2
+    qd = depth // 4
     share = half // 2
     cut = share // 2
     piece = cut // 4
 
     cols = pl.ds(pl.multiple_of(t * half, half), half)
+    first = pl.ds(pl.multiple_of(r * qd, qd), qd)
     loads = []
     for k, (src, dst) in enumerate((
-        (qb_hbm.at[:, cols], base.at[0]), (ob_hbm.at[:, cols], base.at[1]),
+        (qb_hbm.at[first, cols], head), (qb_hbm.at[:, cols], base.at[0]), (ob_hbm.at[:, cols], base.at[1]),
         (qc_hbm, cot.at[0, t]), (ao_hbm, cot.at[1, t]),
         (si_hbm, act.at[0]), (oc_hbm, act.at[1]),
         (mq_hbm, old.at[0]), (mo_hbm, mo),
@@ -131,12 +133,13 @@
             pl.semaphore_signal(barrier, inc=1, device_id=(f, q, s), device_id_type=MESH)
     pl.semaphore_signal(barrier, inc=1, device_id=(f, r, ot), device_id_type=MESH)
 
-    for p in range(2):
-        loads[p].wait()
-        lo, hi = base[p, :, :share], base[p, :, share:]
-        gath[p, f, :, :share] = jnp.concatenate([lo[:, :cut], hi[:, :cut]], axis=1)
-        gath[p, f, :, share:] = jnp.concatenate([lo[:, cut:], hi[:, cut:]], axis=1)
-
+    def deal(p, rows, block):
+        lo, hi = block[:, :share], block[:, share:]
+        gath[p, f, rows, :share] = jnp.concatenate([lo[:, :cut], hi[:, :cut]], axis=1)
+        gath[p, f, rows, share:] = jnp.concatenate([lo[:, cut:], hi[:, cut:]], axis=1)
+
+    loads[0].wait()
+    deal(0, first, head[...])
     pl.semaphore_wait(barrier, 10)
 
     def remote(src, dst, ss, rs, dev):
@@ -149,18 +152,20 @@
 
     h = x * (1 - t) + y * t
     near = rpeer[0] * (1 - t) + rpeer[1] * t
-    mine = pl.ds(pl.multiple_of(h * hd, hd), hd)
-    theirs = pl.ds(pl.multiple_of((1 - h) * hd, hd), hd)
+    mine = (
+        first,
+        pl.ds(pl.multiple_of(h * hd, hd), hd),
+    )
     last = 3
 
-    def unit_ref(u, slab, rows):
+    def unit_ref(u, slab):
         k = u % 2
-        return gath.at[u // 2, slab, rows, k * share : (k + 1) * share]
+        return gath.at[u // 2, slab, mine[u // 2], k * share : (k + 1) * share]
 
     def line(u, way, s, arrive=False):
         step = -1 if way == 0 else 1
         slab = f + step * s + (step if arrive else 0)
-        ref = unit_ref(u, slab, mine)
+        ref = unit_ref(u, slab)
         dev = f + step if arrive else f - step
         to = f if arrive else dev
         slot = s if way == 0 else to + s
@@ -175,15 +180,16 @@
     def carried(way):
         return f if way == 0 else last - f
 
-    def share_slab(u, slab, rows):
-        ref = unit_ref(u, slab, rows)
-        return remote(ref, ref, sent.at[2], aw_r.at[u], (f, near, t))
-
-    def open_line(u, count=None):
+    def share_slab(u, slab):
+        ref = unit_ref(u, slab)
+        for q in (rpeer[2], rpeer[0], rpeer[1]) if u < 2 else (near,):
+            remote(ref, ref, sent.at[2 if u < 2 else 9], aw_r.at[u], (f, q, t)).start()
+
+    def open_line(u, last_only=None):
         for way in range(2):
             go = sends_line(way, 0)
-            if count is not None:
-                go = go & (carried(way) == count)
+            if last_only is not None:
+                go = go & ((carried(way) == 0) == last_only)
 
             @pl.when(go)
             def _():
@@ -202,7 +208,7 @@
             @pl.when(gets_line(way, s))
             def _():
                 slab = f - 1 - s if way == 0 else f + 1 + s
-                share_slab(u, slab, mine).start()
+                share_slab(u, slab)
 
     def swap_cot(p):
         ref = cot.at[p, t]
@@ -212,8 +218,63 @@
         j = 1 - x if k < 2 else x
         c = (0, 1, ot, t)[k]
         return remote(
-            pb.at[u, j, c], t1.at[u, r], sent.at[4], b1_r.at[u], (f, 2 * t + j, c)
+            pb.at[u - 1, j, c], t1.at[u, r], sent.at[4], b1_r.at[u], (f, 2 * t + j, c)
         )
+
+    def scatter_zs():
+        for k in (2, 0, 1):
+            remote(
+                zb.at[fpeer[k]], zt.at[k], sent.at[10], z_r.at[0], (fpeer[k], r, t)
+            ).start()
+
+    def to_owner(k):
+        j = 1 - x if k < 2 else x
+        c = (0, 1, ot, t)[k]
+        return remote(yb.at[j, c], yt.at[r], sent.at[11], z_r.at[1], (f, 2 * t + j, c))
+
+    def scatter_owners():
+        settle(zt, z_r.at[0])
+        total = zb[f].astype(jnp.float32)
+        for k in range(3):
+            total = total + zt[k].astype(jnp.float32)
+        yb[...] = total.astype(jnp.bfloat16)
+        for k in range(3):
+            to_owner(k).start()
+
+        @pl.when(t != y)
+        def _():
+            to_owner(3).start()
+
+        @pl.when(t == y)
+        def _():
+            yt[r] = yb[x, t]
+
+    def spread_own():
+        @pl.when(t != y)
+        def _():
+            settle(yt, z_r.at[1])
+
+        @pl.when(t == y)
+        def _():
+            settle(yt.at[:3], z_r.at[1])
+
+        total = yt[0].astype(jnp.float32)
+        for q in range(1, 4):
+            total = total + yt[q].astype(jnp.float32)
+        send_sums(0, total)
+
+    def spread_sums():
+        for k in range(3):
+            settle(ag.at[2, fsrc[k]], g_r.at[2, k])
+            update_own(2, fsrc[k])
+
+    def spread_zs():
+        rows = rows_at(2, f)
+        settle(full.at[1, :3, rows, :], z_r.at[2])
+        for k in (2, 0, 1):
+            for q in rpeer:
+                ref = full.at[1, q, rows, :]
+                remote(ref, ref, sent.at[12], z_r.at[3], (fpeer[k], r, t)).start()
 
     def slab_dot(p, g, lanes):
         at = pl.ds(pl.multiple_of(g * depth, depth), depth)
@@ -222,20 +283,31 @@
     def project(p, us):
         for u in us:
             k = u % 2
-            settle(gath.at[p, :3, theirs, k * share : (k + 1) * share], aw_r.at[u])
+            settle(
+                gath.at[p, :3, : depth - (qd, hd)[p], k * share : (k + 1) * share], aw_r.at[u]
+            )
         lanes = slice((us[0] % 2) * share, (us[-1] % 2 + 1) * share)
         part = own[p, :, lanes]
         for g in fsrc:
             part = part + slab_dot(p, g, lanes)
         part = part.astype(jnp.bfloat16)
-        for c in range(2):
-            terms = lax.dot_general(
-                part, cot[p, c], (((0,), (0,)), ((), ())), preferred_element_type=jnp.float32
-            )
-            for i, u in enumerate(us):
+        for i, u in reversed(tuple(enumerate(us))):
+            for c in range(2):
+                terms = lax.dot_general(
+                    part[:, i * share : (i + 1) * share], cot[p, c], (((0,), (0,)), ((), ())),
+                    preferred_element_type=jnp.float32,
+                )
                 for j in range(2):
-                    at = i * share + j * cut
-                    pb[u, j, c] = terms[at : at + cut].astype(jnp.bfloat16)
+                    block = terms[j * cut : (j + 1) * cut].astype(jnp.bfloat16)
+                    if u > 0:
+                        pb[u - 1, j, c] = block
+                    else:
+                        for g in range(4):
+                            zb[g, j, c] = block[g * piece : (g + 1) * piece]
+            if u > 0:
+                scatter_reps(u)
+            else:
+                scatter_zs()
 
     def scatter_reps(u):
         for k in range(3):
@@ -247,7 +319,7 @@
 
         @pl.when(t == y)
         def _():
-            t1[u, r] = pb[u, x, t]
+            t1[u, r] = pb[u - 1, x, t]
 
     def scatter_tokens(u):
         @pl.when(t != y)
@@ -277,30 +349,37 @@
 
     def to_dirs(u, g, k):
         ref = full.at[u // 2, r, rows_at(u, g), :]
-        return remote(ref, ref, sent.at[7], d_r.at[u // 2], (f, rpeer[k], t))
+        ss, rs = (sent.at[12], z_r.at[2]) if u == 2 else (sent.at[7], d_r.at[u // 2])
+        return remote(ref, ref, ss, rs, (f, rpeer[k], t))
 
     def to_sums(u, k):
         return remote(
             ag.at[u, f], ag.at[u, f], sent.at[6], g_r.at[u, k], (fpeer[k], r, t)
         )
 
-    def update(u, g):
+    def update_own(u, g):
         p, rows = u // 2, rows_at(u, g)
         new = BETA * old[p, rows, :] + (1.0 - BETA) * ag[u, g].astype(jnp.float32)
         mom[p, rows, :] = new
         full[p, r, rows, :] = new.astype(jnp.bfloat16)
+
+    def update(u, g):
+        update_own(u, g)
         for k in (2, 0, 1):
             to_dirs(u, g, k).start()
+
+    def send_sums(u, total):
+        ag[u, f] = total.astype(jnp.bfloat16)
+        for k in (2, 0, 1):
+            to_sums(u, k).start()
+        update(u, f)
 
     def gather_sums(u):
         total = sb[u, f].astype(jnp.float32)
         settle(t2.at[u], b2_r.at[u])
         for k in range(3):
             total = total + t2[u, k].astype(jnp.float32)
-        ag[u, f] = total.astype(jnp.bfloat16)
-        for k in (2, 0, 1):
-            to_sums(u, k).start()
-        update(u, f)
+        send_sums(u, total)
 
     def gather_dirs(u):
         for k in range(3):
@@ -336,57 +415,61 @@
 
     def finish(p):
         sum_norms(p)
-        settle(full.at[p, :3], d_r.at[p])
+        if p == 0:
+            settle(full.at[0, :3], d_r.at[0])
+        else:
+            settle(full.at[1, :3, : 3 * piece, :], z_r.at[3])
+            settle(full.at[1, :3, :cut, :], d_r.at[1])
 
     open_line(0)
     open_line(1)
-    open_line(2, 0)
-    open_line(3, 0)
+    loads[2].wait()
+    deal(1, slice(None), base[1])
+    open_line(2)
+    open_line(3, True)
+    loads[1].wait()
+    for k in range(1, 4):
+        rows = pl.ds(pl.multiple_of((r + k) % 4 * qd, qd), qd)
+        deal(0, rows, base[0, rows, :])
     for p in range(2):
-        loads[2 + p].wait()
+        loads[3 + p].wait()
         swap_cot(p).start()
-    loads[6].wait()
     loads[7].wait()
+    loads[8].wait()
     old[1] = mo[...].T
     for p in range(2):
-        loads[4 + p].wait()
+        loads[5 + p].wait()
         own[p] = slab_dot(p, f, slice(None))
         settle(cot.at[p, ot], cx_r.at[p])
     run_line(0, 0)
     run_line(1, 0)
-    open_line(2, 1)
+    open_line(3, False)
     run_line(0, 1)
     run_line(1, 1)
-    open_line(2, 2)
+    run_line(2, 0)
     run_line(0, 2)
     run_line(1, 2)
-    run_line(2, 0)
-    open_line(3, 1)
+    run_line(3, 0)
     run_line(2, 1)
-    open_line(3, 2)
-    project(0, (0, 1))
     run_line(2, 2)
-    scatter_reps(0)
-    scatter_reps(1)
-    run_line(3, 0)
-    project(1, (2,))
     run_line(3, 1)
     run_line(3, 2)
-    scatter_reps(2)
-    scatter_tokens(0)
+    project(0, (0, 1))
+    project(1, (2,))
+    project(1, (3,))
     scatter_tokens(1)
-    project(1, (3,))
-    scatter_reps(3)
-    gather_sums(0)
     scatter_tokens(2)
+    scatter_owners()
     gather_sums(1)
     scatter_tokens(3)
+    gather_sums(2)
+    spread_own()
+    gather_dirs(1)
+    gather_sums(3)
+    spread_zs()
+    spread_sums()
     gather_dirs(0)
-    gather_sums(2)
-    gather_dirs(1)
     send_norms(0)
-    gather_sums(3)
-    gather_dirs(2)
     gather_dirs(3)
     send_norms(1)
     finish(0)
@@ -395,28 +478,33 @@
 
     @pl.when(inner)
     def _():
-        settle(gath.at[0, :2], sent.at[0])
-        settle(gath.at[0, :3], sent.at[1])
+        settle(gath.at[0, :3, :, :share], sent.at[0])
+        settle(gath.at[0, :3, : depth - qd], sent.at[1])
 
     @pl.when(jnp.logical_not(inner))
     def _():
-        settle(gath.at[0, :1], sent.at[0])
-
-    settle(gath.at[0, :3], sent.at[2])
+        settle(gath.at[0, :3, :hd, :share], sent.at[0])
+
+    for k in range(2):
+        settle(gath.at[k, :3, : depth - (qd, hd)[k], :], sent.at[2 + 7 * k])
     settle(cot.at[0], sent.at[3])
 
     @pl.when(t != y)
     def _():
         settle(pb, sent.at[4])
+        settle(yt, sent.at[11])
 
     @pl.when(t == y)
     def _():
-        settle(pb.at[:3], sent.at[4])
-
-    settle(t2, sent.at[5])
+        settle(pb.at[:, :, :, : 3 * piece], sent.at[4])
+        settle(yt.at[:3], sent.at[11])
+
+    settle(t2.at[:3], sent.at[5])
     settle(t2, sent.at[6])
-    settle(full.at[:, :3], sent.at[7])
+    settle(full.at[:, :3, : 6 * piece], sent.at[7])
     settle(nrm.at[:, :7], sent.at[8])
+    settle(zt, sent.at[10])
+    settle(t2, sent.at[12])
 
 
 def finish_kernel(
@@ -473,26 +561,31 @@
         scratch_shapes=[
             pltpu.VMEM((2, tokens, depth_all), bf),
             pltpu.VMEM((2, 2, tokens, width), bf),
+            pltpu.VMEM((depth // 4, rank // 2), bf),
             pltpu.VMEM((2, depth, rank // 2), bf),
             pltpu.VMEM((2, share, width), f32),
             pltpu.VMEM((width, share), f32),
             pltpu.VMEM((2, 4, depth, 2 * share), bf),
             pltpu.VMEM((2, tokens, 2 * share), f32),
-            pltpu.VMEM((UNITS, 2, 2, cut, width), bf),
+            pltpu.VMEM((UNITS - 1, 2, 2, cut, width), bf),
             pltpu.VMEM((UNITS, 4, cut, width), bf),
             pltpu.VMEM((UNITS, 4, piece, width), bf),
             pltpu.VMEM((UNITS, 3, piece, width), bf),
             pltpu.VMEM((UNITS, 4, piece, width), bf),
             pltpu.VMEM((2, 8, 8, 128), f32),
-            dma((8,)), dma((9,)), dma((2,)), dma((UNITS, 3)), dma((UNITS,)), dma((UNITS,)),
-            dma((UNITS,)), dma((UNITS, 3)), dma((2,)), dma((2,)),
+            pltpu.VMEM((4, 2, 2, piece, width), bf),
+            pltpu.VMEM((3, 2, 2, piece, width), bf),
+            pltpu.VMEM((2, 2, piece, width), bf),
+            pltpu.VMEM((4, piece, width), bf),
+            dma((9,)), dma((13,)), dma((2,)), dma((UNITS, 3)), dma((UNITS,)), dma((UNITS,)),
+            dma((UNITS,)), dma((UNITS, 3)), dma((2,)), dma((2,)), dma((4,)),
         ],
         compiler_params=pltpu.CompilerParams(
             collective_id=0, has_side_effects=True, vmem_limit_bytes=20 * 2**20
         ),
     )(*(pltpu.with_memory_space_constraint(a, pltpu.HBM) for a in ins))
     full = full.reshape(2, rank, width)
-    n = 4
+    n = 2
     rows = pl.BlockSpec((depth // n, rank), lambda i: (i, 0))
     whole = pl.BlockSpec((depth, rank), lambda i: (0, 0))
     wq = pl.BlockSpec((depth // n, width), lambda i: (i, 0))

time: 56.7 us -> 51.7 us (0.912)
  Pallas kernels: 55.8 us -> 50.8 us
    pallas_call x1, Pallas kernels: 52.4 us -> 47.9 us  [on_device_fast(): pl.pallas_call(exchange_kernel, out_shape=(jax.ShapeDtypeStruct((2, 4, sh...]
where the time goes in v3:
time: 51.7 us; the launch traced here: 51.5 us
  Pallas kernels  50.8 us (98%)
  between operations  0.71 us (1%)
    pallas_call x1, Pallas kernels, on_device_fast(): pl.pallas_call(exchange_kernel, out_shape=(jax.ShapeDtypeStruct((2, 4, sh...  47.9 us
    pallas_call x1, Pallas kernels, on_device_fast(): pl.pallas_call(functools.partial(finish_kernel, entries), grid=(n,), out_...  2.94 us

profile of v3, /device:TPU:0, one launch (start us, length us, event | category | flops | bytes accessed | tf_op | source)
XLA Modules:
  0.0 51.5 jit_solution(6582408755932321322)
XLA Ops:
  0.6 0.0 copy-start.1
  0.6 0.0 copy-start
  0.7 0.0 copy-start.3
  0.7 0.0 copy-start.2
  0.7 47.9 %shard_map.161 = (bf16[2,4,128,512]{3,2,1,0:T(8,128)(2,1)S(1)}, f32[2,128,512]{2,1,0:T(8,128)S(1)}, f32[2,8,128]{2,1,0:T(8,128)S(1)}) custom-call(bf16[352,2048]{1,0:T(8,128)(2,1)} %si_hbm.1, bf16[352,2048]{1,0:T(8,128)(2,1)} %oc_hbm.1, bf16[352,512]{1,0:T(8,128)(2,1)} %qc_hbm.1, bf16[352,512]{1,0:T(8,128)(2,1)} %ao_hbm.1, bf16[512,512]{1,0:T(8,128)(2,1)} %qb.1, ...), custom_call_target="tpu_custom_call" | custom-call | tf_op jit(solution)/shard_map/pallas_call | solution.py:552
  48.6 0.0 copy-done.1
  48.6 0.0 copy-done
  48.6 0.0 copy-done.3
  48.6 0.0 copy-done.2
  48.6 2.9 %shard_map.162 = (f32[512,512]{1,0:T(8,128)}, f32[512,512]{1,0:T(8,128)}, f32[512,512]{1,0:T(8,128)}, f32[512,512]{1,0:T(8,128)}, bf16[512,512]{1,0:T(8,128)(2,1...) custom-call(bf16[512,512]{1,0:T(8,128)(2,1)S(1)} %copy-done, bf16[512,512]{1,0:T(8,128)(2,1)S(1)} %copy-done.1, ...), custom_call_target="tpu_custom_call" | custom-call | flops 536870912 | bytes 5242880 | tf_op jit(solution)/shard_map/pallas_call | solution.py:596
Async XLA Ops:
  0.6 47.9 %copy-start.1 = (bf16[512,512]{1,0:T(8,128)(2,1)S(1)}, bf16[512,512]{1,0:T(8,128)(2,1)}, u32[]{:S(2)}) copy-start(bf16[512,512]{1,0:T(8,128)(2,1)} %ob.1) | copy-start | bytes 1572868
  0.6 47.9 %copy-start = (bf16[512,512]{1,0:T(8,128)(2,1)S(1)}, bf16[512,512]{1,0:T(8,128)(2,1)}, u32[]{:S(2)}) copy-start(bf16[512,512]{1,0:T(8,128)(2,1)} %qb.1) | copy-start | bytes 1572868
  0.7 47.9 %copy-start.3 = (f32[512,512]{1,0:T(8,128)S(1)}, f32[512,512]{1,0:T(8,128)}, u32[]{:S(2)}) copy-start(f32[512,512]{1,0:T(8,128)} %ow.1) | copy-start | bytes 3145732
  0.7 47.9 %copy-start.2 = (f32[512,512]{1,0:T(8,128)S(1)}, f32[512,512]{1,0:T(8,128)}, u32[]{:S(2)}) copy-start(f32[512,512]{1,0:T(8,128)} %qw.1) | copy-start | bytes 3145732

commit v4 on v3

--- a/solution.py
+++ b/solution.py
@@ -102,8 +102,7 @@
     f, r, t = lax.axis_index("fs"), lax.axis_index("rep"), lax.axis_index("tp")
     y, x = r // 2, r % 2
     ot = 1 - t
-    fpeer = [(f + d) % 4 for d in (1, 3, 2)]
-    fsrc = [(f + 4 - d) % 4 for d in (1, 3, 2)]
+    fpeer = [3 - f, (f + 2) % 4, f + 1 - 2 * (f % 2)]
     rpeer = [2 * y + (1 - x), 2 * (1 - y) + x, 3 - r]
     depth, half = base.shape[1], base.shape[2]
     hd = depth // 2
@@ -180,10 +179,10 @@
     def carried(way):
         return f if way == 0 else last - f
 
-    def share_slab(u, slab):
+    def share_slab(u, slab, slot):
         ref = unit_ref(u, slab)
         for q in (rpeer[2], rpeer[0], rpeer[1]) if u < 2 else (near,):
-            remote(ref, ref, sent.at[2 if u < 2 else 9], aw_r.at[u], (f, q, t)).start()
+            remote(ref, ref, sent.at[2 if u < 2 else 9], aw_r.at[max(u - 1, 0), slot], (f, q, t)).start()
 
     def open_line(u, last_only=None):
         for way in range(2):
@@ -208,7 +207,7 @@
             @pl.when(gets_line(way, s))
             def _():
                 slab = f - 1 - s if way == 0 else f + 1 + s
-                share_slab(u, slab)
+                share_slab(u, slab, s if way == 0 else f + s)
 
     def swap_cot(p):
         ref = cot.at[p, t]
@@ -222,7 +221,7 @@
         )
 
     def scatter_zs():
-        for k in (2, 0, 1):
+        for k in range(3):
             remote(
                 zb.at[fpeer[k]], zt.at[k], sent.at[10], z_r.at[0], (fpeer[k], r, t)
             ).start()
@@ -264,14 +263,14 @@
         send_sums(0, total)
 
     def spread_sums():
-        for k in range(3):
-            settle(ag.at[2, fsrc[k]], g_r.at[2, k])
-            update_own(2, fsrc[k])
+        for k in (2, 1, 0):
+            settle(ag.at[2, fpeer[k]], g_r.at[2, k])
+            update_own(2, fpeer[k])
 
     def spread_zs():
         rows = rows_at(2, f)
         settle(full.at[1, :3, rows, :], z_r.at[2])
-        for k in (2, 0, 1):
+        for k in range(3):
             for q in rpeer:
                 ref = full.at[1, q, rows, :]
                 remote(ref, ref, sent.at[12], z_r.at[3], (fpeer[k], r, t)).start()
@@ -280,16 +279,20 @@
         at = pl.ds(pl.multiple_of(g * depth, depth), depth)
         return jnp.dot(act[p, :, at], gath[p, g, :, lanes], preferred_element_type=jnp.float32)
 
+    def lanes_of(us):
+        return slice((us[0] % 2) * share, (us[-1] % 2 + 1) * share)
+
+    def partial(p, us, slot):
+        lanes = lanes_of(us)
+        settle(gath.at[p, 0, : depth - (qd, hd)[p], lanes], aw_r.at[max(us[0] - 1, 0), slot])
+        slab = jnp.where(slot < f, f - 1 - slot, slot + 1)
+        return own[p, :, lanes] + slab_dot(p, slab, lanes)
+
+    def prepare(p, us, slot):
+        own[p, :, lanes_of(us)] = partial(p, us, slot)
+
     def project(p, us):
-        for u in us:
-            k = u % 2
-            settle(
-                gath.at[p, :3, : depth - (qd, hd)[p], k * share : (k + 1) * share], aw_r.at[u]
-            )
-        lanes = slice((us[0] % 2) * share, (us[-1] % 2 + 1) * share)
-        part = own[p, :, lanes]
-        for g in fsrc:
-            part = part + slab_dot(p, g, lanes)
+        part = partial(p, us, 2)
         part = part.astype(jnp.bfloat16)
         for i, u in reversed(tuple(enumerate(us))):
             for c in range(2):
@@ -335,7 +338,7 @@
             total = total + t1[u, q].astype(jnp.float32)
         for g in range(4):
             sb[u, g] = total[g * piece : (g + 1) * piece].astype(jnp.bfloat16)
-        for k in (2, 0, 1):
+        for k in range(3):
             to_token(u, k).start()
 
     def to_token(u, k):
@@ -370,7 +373,7 @@
 
     def send_sums(u, total):
         ag[u, f] = total.astype(jnp.bfloat16)
-        for k in (2, 0, 1):
+        for k in range(3):
             to_sums(u, k).start()
         update(u, f)
 
@@ -382,9 +385,9 @@
         send_sums(u, total)
 
     def gather_dirs(u):
-        for k in range(3):
-            settle(ag.at[u, fsrc[k]], g_r.at[u, k])
-            update(u, fsrc[k])
+        for k in (2, 1, 0):
+            settle(ag.at[u, fpeer[k]], g_r.at[u, k])
+            update(u, fpeer[k])
 
     others = [(q, s) for q in rpeer for s in (t, ot)] + [(r, ot)]
     me = 2 * r + t
@@ -451,11 +454,17 @@
     run_line(1, 2)
     run_line(3, 0)
     run_line(2, 1)
+    run_line(3, 1)
+    prepare(0, (0, 1), 0)
+    prepare(0, (0, 1), 1)
     run_line(2, 2)
-    run_line(3, 1)
+    prepare(1, (2,), 0)
     run_line(3, 2)
     project(0, (0, 1))
+    prepare(1, (2,), 1)
     project(1, (2,))
+    prepare(1, (3,), 0)
+    prepare(1, (3,), 1)
     project(1, (3,))
     scatter_tokens(1)
     scatter_tokens(2)
@@ -577,7 +586,7 @@
             pltpu.VMEM((3, 2, 2, piece, width), bf),
             pltpu.VMEM((2, 2, piece, width), bf),
             pltpu.VMEM((4, piece, width), bf),
-            dma((9,)), dma((13,)), dma((2,)), dma((UNITS, 3)), dma((UNITS,)), dma((UNITS,)),
+            dma((9,)), dma((13,)), dma((2,)), dma((UNITS, 3)), dma((3, 3)), dma((UNITS,)),
             dma((UNITS,)), dma((UNITS, 3)), dma((2,)), dma((2,)), dma((4,)),
         ],
         compiler_params=pltpu.CompilerParams(

time: 51.7 us -> 49.7 us (0.961)
  Pallas kernels: 50.8 us -> 48.8 us
    pallas_call x1, Pallas kernels: 47.9 us -> 45.9 us  [on_device_fast(): pl.pallas_call(exchange_kernel, out_shape=(jax.ShapeDtypeStruct((2, 4, sh...]
where the time goes in v4:
time: 49.7 us; the launch traced here: 49.5 us
  Pallas kernels  48.8 us (98%)
  between operations  0.71 us (1%)
    pallas_call x1, Pallas kernels, on_device_fast(): pl.pallas_call(exchange_kernel, out_shape=(jax.ShapeDtypeStruct((2, 4, sh...  45.9 us
    pallas_call x1, Pallas kernels, on_device_fast(): pl.pallas_call(functools.partial(finish_kernel, entries), grid=(n,), out_...  2.94 us

profile of v4, /device:TPU:0, one launch (start us, length us, event | category | flops | bytes accessed | tf_op | source)
XLA Modules:
  0.0 49.5 jit_solution(16198665980582222047)
XLA Ops:
  0.6 0.0 copy-start.1
  0.6 0.0 copy-start
  0.7 0.0 copy-start.3
  0.7 0.0 copy-start.2
  0.7 45.9 %shard_map.161 = (bf16[2,4,128,512]{3,2,1,0:T(8,128)(2,1)S(1)}, f32[2,128,512]{2,1,0:T(8,128)S(1)}, f32[2,8,128]{2,1,0:T(8,128)S(1)}) custom-call(bf16[352,2048]{1,0:T(8,128)(2,1)} %si_hbm.1, bf16[352,2048]{1,0:T(8,128)(2,1)} %oc_hbm.1, bf16[352,512]{1,0:T(8,128)(2,1)} %qc_hbm.1, bf16[352,512]{1,0:T(8,128)(2,1)} %ao_hbm.1, bf16[512,512]{1,0:T(8,128)(2,1)} %qb.1, ...), custom_call_target="tpu_custom_call" | custom-call | tf_op jit(solution)/shard_map/pallas_call | solution.py:561
  46.6 0.0 copy-done.1
  46.6 0.0 copy-done
  46.6 0.0 copy-done.3
  46.6 0.0 copy-done.2
  46.6 2.9 %shard_map.162 = (f32[512,512]{1,0:T(8,128)}, f32[512,512]{1,0:T(8,128)}, f32[512,512]{1,0:T(8,128)}, f32[512,512]{1,0:T(8,128)}, bf16[512,512]{1,0:T(8,128)(2,1...) custom-call(bf16[512,512]{1,0:T(8,128)(2,1)S(1)} %copy-done, bf16[512,512]{1,0:T(8,128)(2,1)S(1)} %copy-done.1, ...), custom_call_target="tpu_custom_call" | custom-call | flops 536870912 | bytes 5242880 | tf_op jit(solution)/shard_map/pallas_call | solution.py:605
Async XLA Ops:
  0.6 45.9 %copy-start.1 = (bf16[512,512]{1,0:T(8,128)(2,1)S(1)}, bf16[512,512]{1,0:T(8,128)(2,1)}, u32[]{:S(2)}) copy-start(bf16[512,512]{1,0:T(8,128)(2,1)} %ob.1) | copy-start | bytes 1572868
  0.6 45.9 %copy-start = (bf16[512,512]{1,0:T(8,128)(2,1)S(1)}, bf16[512,512]{1,0:T(8,128)(2,1)}, u32[]{:S(2)}) copy-start(bf16[512,512]{1,0:T(8,128)(2,1)} %qb.1) | copy-start | bytes 1572868
  0.7 45.9 %copy-start.3 = (f32[512,512]{1,0:T(8,128)S(1)}, f32[512,512]{1,0:T(8,128)}, u32[]{:S(2)}) copy-start(f32[512,512]{1,0:T(8,128)} %ow.1) | copy-start | bytes 3145732
  0.7 45.9 %copy-start.2 = (f32[512,512]{1,0:T(8,128)S(1)}, f32[512,512]{1,0:T(8,128)}, u32[]{:S(2)}) copy-start(f32[512,512]{1,0:T(8,128)} %qw.1) | copy-start | bytes 3145732

commit v5 on v4

--- a/solution.py
+++ b/solution.py
@@ -291,7 +291,7 @@
     def prepare(p, us, slot):
         own[p, :, lanes_of(us)] = partial(p, us, slot)
 
-    def project(p, us):
+    def project(p, us, between=None):
         part = partial(p, us, 2)
         part = part.astype(jnp.bfloat16)
         for i, u in reversed(tuple(enumerate(us))):
@@ -307,6 +307,8 @@
                     else:
                         for g in range(4):
                             zb[g, j, c] = block[g * piece : (g + 1) * piece]
+            if between is not None and u == us[-1]:
+                between()
             if u > 0:
                 scatter_reps(u)
             else:
@@ -458,9 +460,8 @@
     prepare(0, (0, 1), 0)
     prepare(0, (0, 1), 1)
     run_line(2, 2)
+    project(0, (0, 1), lambda: run_line(3, 2))
     prepare(1, (2,), 0)
-    run_line(3, 2)
-    project(0, (0, 1))
     prepare(1, (2,), 1)
     project(1, (2,))
     prepare(1, (3,), 0)

time: 49.7 us -> 51.4 us (1.034)
  Pallas kernels: 48.8 us -> 50.5 us
    pallas_call x1, Pallas kernels: 45.9 us -> 47.6 us  [on_device_fast(): pl.pallas_call(exchange_kernel, out_shape=(jax.ShapeDtypeStruct((2, 4, sh...]
where the time goes in v5:
time: 51.4 us; the launch traced here: 51.3 us
  Pallas kernels  50.5 us (98%)
  between operations  0.71 us (1%)
    pallas_call x1, Pallas kernels, on_device_fast(): pl.pallas_call(exchange_kernel, out_shape=(jax.ShapeDtypeStruct((2, 4, sh...  47.6 us
    pallas_call x1, Pallas kernels, on_device_fast(): pl.pallas_call(functools.partial(finish_kernel, entries), grid=(n,), out_...  2.94 us

profile of v5, /device:TPU:0, one launch (start us, length us, event | category | flops | bytes accessed | tf_op | source)
XLA Modules:
  0.0 51.3 jit_solution(3050196891078551769)
XLA Ops:
  0.6 0.0 copy-start.1
  0.6 0.0 copy-start
  0.7 0.0 copy-start.3
  0.7 0.0 copy-start.2
  0.7 47.6 %shard_map.161 = (bf16[2,4,128,512]{3,2,1,0:T(8,128)(2,1)S(1)}, f32[2,128,512]{2,1,0:T(8,128)S(1)}, f32[2,8,128]{2,1,0:T(8,128)S(1)}) custom-call(bf16[352,2048]{1,0:T(8,128)(2,1)} %si_hbm.1, bf16[352,2048]{1,0:T(8,128)(2,1)} %oc_hbm.1, bf16[352,512]{1,0:T(8,128)(2,1)} %qc_hbm.1, bf16[352,512]{1,0:T(8,128)(2,1)} %ao_hbm.1, bf16[512,512]{1,0:T(8,128)(2,1)} %qb.1, ...), custom_call_target="tpu_custom_call" | custom-call | tf_op jit(solution)/shard_map/pallas_call | solution.py:562
  48.3 0.0 copy-done.1
  48.3 0.0 copy-done
  48.3 0.0 copy-done.3
  48.3 0.0 copy-done.2
  48.3 2.9 %shard_map.162 = (f32[512,512]{1,0:T(8,128)}, f32[512,512]{1,0:T(8,128)}, f32[512,512]{1,0:T(8,128)}, f32[512,512]{1,0:T(8,128)}, bf16[512,512]{1,0:T(8,128)(2,1...) custom-call(bf16[512,512]{1,0:T(8,128)(2,1)S(1)} %copy-done, bf16[512,512]{1,0:T(8,128)(2,1)S(1)} %copy-done.1, ...), custom_call_target="tpu_custom_call" | custom-call | flops 536870912 | bytes 5242880 | tf_op jit(solution)/shard_map/pallas_call | solution.py:606
Async XLA Ops:
  0.6 47.6 %copy-start.1 = (bf16[512,512]{1,0:T(8,128)(2,1)S(1)}, bf16[512,512]{1,0:T(8,128)(2,1)}, u32[]{:S(2)}) copy-start(bf16[512,512]{1,0:T(8,128)(2,1)} %ob.1) | copy-start | bytes 1572868
  0.6 47.6 %copy-start = (bf16[512,512]{1,0:T(8,128)(2,1)S(1)}, bf16[512,512]{1,0:T(8,128)(2,1)}, u32[]{:S(2)}) copy-start(bf16[512,512]{1,0:T(8,128)(2,1)} %qb.1) | copy-start | bytes 1572868
  0.7 47.6 %copy-start.3 = (f32[512,512]{1,0:T(8,128)S(1)}, f32[512,512]{1,0:T(8,128)}, u32[]{:S(2)}) copy-start(f32[512,512]{1,0:T(8,128)} %ow.1) | copy-start | bytes 3145732
  0.7 47.6 %copy-start.2 = (f32[512,512]{1,0:T(8,128)S(1)}, f32[512,512]{1,0:T(8,128)}, u32[]{:S(2)}) copy-start(f32[512,512]{1,0:T(8,128)} %qw.1) | copy-start | bytes 3145732

commit v6 on v4

--- a/solution.py
+++ b/solution.py
@@ -182,7 +182,7 @@
     def share_slab(u, slab, slot):
         ref = unit_ref(u, slab)
         for q in (rpeer[2], rpeer[0], rpeer[1]) if u < 2 else (near,):
-            remote(ref, ref, sent.at[2 if u < 2 else 9], aw_r.at[max(u - 1, 0), slot], (f, q, t)).start()
+            remote(ref, ref, sent.at[2 if u < 2 else 9], aw_r.at[u, slot], (f, q, t)).start()
 
     def open_line(u, last_only=None):
         for way in range(2):
@@ -269,11 +269,11 @@
 
     def spread_zs():
         rows = rows_at(2, f)
-        settle(full.at[1, :3, rows, :], z_r.at[2])
-        for k in range(3):
-            for q in rpeer:
-                ref = full.at[1, q, rows, :]
-                remote(ref, ref, sent.at[12], z_r.at[3], (fpeer[k], r, t)).start()
+        for j in range(3):
+            ref = full.at[1, rpeer[j], rows, :]
+            settle(ref, z_r.at[2 + j])
+            for k in range(3):
+                remote(ref, ref, sent.at[12], z_r.at[5], (fpeer[k], r, t)).start()
 
     def slab_dot(p, g, lanes):
         at = pl.ds(pl.multiple_of(g * depth, depth), depth)
@@ -284,7 +284,7 @@
 
     def partial(p, us, slot):
         lanes = lanes_of(us)
-        settle(gath.at[p, 0, : depth - (qd, hd)[p], lanes], aw_r.at[max(us[0] - 1, 0), slot])
+        settle(gath.at[p, 0, : depth - (qd, hd)[p], lanes], aw_r.at[us[0], slot])
         slab = jnp.where(slot < f, f - 1 - slot, slot + 1)
         return own[p, :, lanes] + slab_dot(p, slab, lanes)
 
@@ -352,7 +352,7 @@
 
     def to_dirs(u, g, k):
         ref = full.at[u // 2, r, rows_at(u, g), :]
-        ss, rs = (sent.at[12], z_r.at[2]) if u == 2 else (sent.at[7], d_r.at[u // 2])
+        ss, rs = (sent.at[12], z_r.at[2 + k]) if u == 2 else (sent.at[7], d_r.at[u // 2])
         return remote(ref, ref, ss, rs, (f, rpeer[k], t))
 
     def to_sums(u, k):
@@ -421,11 +421,11 @@
         if p == 0:
             settle(full.at[0, :3], d_r.at[0])
         else:
-            settle(full.at[1, :3, : 3 * piece, :], z_r.at[3])
+            settle(full.at[1, :3, : 3 * piece, :], z_r.at[5])
             settle(full.at[1, :3, :cut, :], d_r.at[1])
 
+    open_line(1)
     open_line(0)
-    open_line(1)
     loads[2].wait()
     deal(1, slice(None), base[1])
     open_line(2)
@@ -444,41 +444,44 @@
         loads[5 + p].wait()
         own[p] = slab_dot(p, f, slice(None))
         settle(cot.at[p, ot], cx_r.at[p])
+    run_line(1, 0)
     run_line(0, 0)
-    run_line(1, 0)
     open_line(3, False)
+    run_line(1, 1)
     run_line(0, 1)
-    run_line(1, 1)
     run_line(2, 0)
+    run_line(1, 2)
     run_line(0, 2)
-    run_line(1, 2)
     run_line(3, 0)
     run_line(2, 1)
     run_line(3, 1)
-    prepare(0, (0, 1), 0)
-    prepare(0, (0, 1), 1)
+    prepare(0, (1,), 0)
+    prepare(0, (0,), 0)
+    prepare(0, (1,), 1)
     run_line(2, 2)
+    prepare(0, (0,), 1)
+    project(0, (1,))
+    run_line(3, 2)
+    project(0, (0,))
     prepare(1, (2,), 0)
-    run_line(3, 2)
-    project(0, (0, 1))
     prepare(1, (2,), 1)
     project(1, (2,))
     prepare(1, (3,), 0)
     prepare(1, (3,), 1)
     project(1, (3,))
     scatter_tokens(1)
+    scatter_owners()
     scatter_tokens(2)
-    scatter_owners()
     gather_sums(1)
     scatter_tokens(3)
+    spread_own()
     gather_sums(2)
-    spread_own()
     gather_dirs(1)
     gather_sums(3)
+    gather_dirs(0)
+    send_norms(0)
     spread_zs()
     spread_sums()
-    gather_dirs(0)
-    send_norms(0)
     gather_dirs(3)
     send_norms(1)
     finish(0)
@@ -586,8 +589,8 @@
             pltpu.VMEM((3, 2, 2, piece, width), bf),
             pltpu.VMEM((2, 2, piece, width), bf),
             pltpu.VMEM((4, piece, width), bf),
-            dma((9,)), dma((13,)), dma((2,)), dma((UNITS, 3)), dma((3, 3)), dma((UNITS,)),
-            dma((UNITS,)), dma((UNITS, 3)), dma((2,)), dma((2,)), dma((4,)),
+            dma((9,)), dma((13,)), dma((2,)), dma((UNITS, 3)), dma((UNITS, 3)), dma((UNITS,)),
+            dma((UNITS,)), dma((UNITS, 3)), dma((2,)), dma((2,)), dma((6,)),
         ],
         compiler_params=pltpu.CompilerParams(
             collective_id=0, has_side_effects=True, vmem_limit_bytes=20 * 2**20

time: 49.7 us -> 49.1 us (0.988)
  Pallas kernels: 48.8 us -> 48.2 us
    pallas_call x1, Pallas kernels: 45.9 us -> 45.3 us  [on_device_fast(): pl.pallas_call(exchange_kernel, out_shape=(jax.ShapeDtypeStruct((2, 4, sh...]
where the time goes in v6:
time: 49.1 us; the launch traced here: 49 us
  Pallas kernels  48.2 us (98%)
  between operations  0.71 us (1%)
    pallas_call x1, Pallas kernels, on_device_fast(): pl.pallas_call(exchange_kernel, out_shape=(jax.ShapeDtypeStruct((2, 4, sh...  45.3 us
    pallas_call x1, Pallas kernels, on_device_fast(): pl.pallas_call(functools.partial(finish_kernel, entries), grid=(n,), out_...  2.94 us

profile of v6, /device:TPU:0, one launch (start us, length us, event | category | flops | bytes accessed | tf_op | source)
XLA Modules:
  0.0 49.0 jit_solution(6337084870955931871)
XLA Ops:
  0.6 0.0 copy-start.1
  0.6 0.0 copy-start
  0.7 0.0 copy-start.3
  0.7 0.0 copy-start.2
  0.7 45.3 %shard_map.161 = (bf16[2,4,128,512]{3,2,1,0:T(8,128)(2,1)S(1)}, f32[2,128,512]{2,1,0:T(8,128)S(1)}, f32[2,8,128]{2,1,0:T(8,128)S(1)}) custom-call(bf16[352,2048]{1,0:T(8,128)(2,1)} %si_hbm.1, bf16[352,2048]{1,0:T(8,128)(2,1)} %oc_hbm.1, bf16[352,512]{1,0:T(8,128)(2,1)} %qc_hbm.1, bf16[352,512]{1,0:T(8,128)(2,1)} %ao_hbm.1, bf16[512,512]{1,0:T(8,128)(2,1)} %qb.1, ...), custom_call_target="tpu_custom_call" | custom-call | tf_op jit(solution)/shard_map/pallas_call | solution.py:564
  46.0 0.0 copy-done.1
  46.0 0.0 copy-done
  46.0 0.0 copy-done.3
  46.0 0.0 copy-done.2
  46.0 2.9 %shard_map.162 = (f32[512,512]{1,0:T(8,128)}, f32[512,512]{1,0:T(8,128)}, f32[512,512]{1,0:T(8,128)}, f32[512,512]{1,0:T(8,128)}, bf16[512,512]{1,0:T(8,128)(2,1...) custom-call(bf16[512,512]{1,0:T(8,128)(2,1)S(1)} %copy-done, bf16[512,512]{1,0:T(8,128)(2,1)S(1)} %copy-done.1, ...), custom_call_target="tpu_custom_call" | custom-call | flops 536870912 | bytes 5242880 | tf_op jit(solution)/shard_map/pallas_call | solution.py:608
Async XLA Ops:
  0.6 45.4 %copy-start.1 = (bf16[512,512]{1,0:T(8,128)(2,1)S(1)}, bf16[512,512]{1,0:T(8,128)(2,1)}, u32[]{:S(2)}) copy-start(bf16[512,512]{1,0:T(8,128)(2,1)} %ob.1) | copy-start | bytes 1572868
  0.6 45.4 %copy-start = (bf16[512,512]{1,0:T(8,128)(2,1)S(1)}, bf16[512,512]{1,0:T(8,128)(2,1)}, u32[]{:S(2)}) copy-start(bf16[512,512]{1,0:T(8,128)(2,1)} %qb.1) | copy-start | bytes 1572868
  0.7 45.4 %copy-start.3 = (f32[512,512]{1,0:T(8,128)S(1)}, f32[512,512]{1,0:T(8,128)}, u32[]{:S(2)}) copy-start(f32[512,512]{1,0:T(8,128)} %ow.1) | copy-start | bytes 3145732
  0.7 45.4 %copy-start.2 = (f32[512,512]{1,0:T(8,128)S(1)}, f32[512,512]{1,0:T(8,128)}, u32[]{:S(2)}) copy-start(f32[512,512]{1,0:T(8,128)} %qw.1) | copy-start | bytes 3145732

commit v7 on v6

--- a/solution.py
+++ b/solution.py
@@ -459,9 +459,9 @@
     prepare(0, (0,), 0)
     prepare(0, (1,), 1)
     run_line(2, 2)
-    prepare(0, (0,), 1)
     project(0, (1,))
     run_line(3, 2)
+    prepare(0, (0,), 1)
     project(0, (0,))
     prepare(1, (2,), 0)
     prepare(1, (2,), 1)

time: 49.1 us -> 49.7 us (1.012)
  Pallas kernels: 48.2 us -> 48.8 us
    pallas_call x1, Pallas kernels: 45.3 us -> 45.9 us  [on_device_fast(): pl.pallas_call(exchange_kernel, out_shape=(jax.ShapeDtypeStruct((2, 4, sh...]
where the time goes in v7:
time: 49.7 us; the launch traced here: 49.6 us
  Pallas kernels  48.8 us (98%)
  between operations  0.71 us (1%)
    pallas_call x1, Pallas kernels, on_device_fast(): pl.pallas_call(exchange_kernel, out_shape=(jax.ShapeDtypeStruct((2, 4, sh...  45.9 us
    pallas_call x1, Pallas kernels, on_device_fast(): pl.pallas_call(functools.partial(finish_kernel, entries), grid=(n,), out_...  2.94 us

profile of v7, /device:TPU:0, one launch (start us, length us, event | category | flops | bytes accessed | tf_op | source)
XLA Modules:
  0.0 49.6 jit_solution(12784468423683452375)
XLA Ops:
  0.6 0.0 copy-start.1
  0.6 0.0 copy-start
  0.7 0.0 copy-start.3
  0.7 0.0 copy-start.2
  0.7 45.9 %shard_map.161 = (bf16[2,4,128,512]{3,2,1,0:T(8,128)(2,1)S(1)}, f32[2,128,512]{2,1,0:T(8,128)S(1)}, f32[2,8,128]{2,1,0:T(8,128)S(1)}) custom-call(bf16[352,2048]{1,0:T(8,128)(2,1)} %si_hbm.1, bf16[352,2048]{1,0:T(8,128)(2,1)} %oc_hbm.1, bf16[352,512]{1,0:T(8,128)(2,1)} %qc_hbm.1, bf16[352,512]{1,0:T(8,128)(2,1)} %ao_hbm.1, bf16[512,512]{1,0:T(8,128)(2,1)} %qb.1, ...), custom_call_target="tpu_custom_call" | custom-call | tf_op jit(solution)/shard_map/pallas_call | solution.py:564
  46.6 0.0 copy-done.1
  46.6 0.0 copy-done
  46.6 0.0 copy-done.3
  46.6 0.0 copy-done.2
  46.6 2.9 %shard_map.162 = (f32[512,512]{1,0:T(8,128)}, f32[512,512]{1,0:T(8,128)}, f32[512,512]{1,0:T(8,128)}, f32[512,512]{1,0:T(8,128)}, bf16[512,512]{1,0:T(8,128)(2,1...) custom-call(bf16[512,512]{1,0:T(8,128)(2,1)S(1)} %copy-done, bf16[512,512]{1,0:T(8,128)(2,1)S(1)} %copy-done.1, ...), custom_call_target="tpu_custom_call" | custom-call | flops 536870912 | bytes 5242880 | tf_op jit(solution)/shard_map/pallas_call | solution.py:608
Async XLA Ops:
  0.6 45.9 %copy-start.1 = (bf16[512,512]{1,0:T(8,128)(2,1)S(1)}, bf16[512,512]{1,0:T(8,128)(2,1)}, u32[]{:S(2)}) copy-start(bf16[512,512]{1,0:T(8,128)(2,1)} %ob.1) | copy-start | bytes 1572868
  0.6 45.9 %copy-start = (bf16[512,512]{1,0:T(8,128)(2,1)S(1)}, bf16[512,512]{1,0:T(8,128)(2,1)}, u32[]{:S(2)}) copy-start(bf16[512,512]{1,0:T(8,128)(2,1)} %qb.1) | copy-start | bytes 1572868
  0.7 45.9 %copy-start.3 = (f32[512,512]{1,0:T(8,128)S(1)}, f32[512,512]{1,0:T(8,128)}, u32[]{:S(2)}) copy-start(f32[512,512]{1,0:T(8,128)} %ow.1) | copy-start | bytes 3145732
  0.7 45.9 %copy-start.2 = (f32[512,512]{1,0:T(8,128)S(1)}, f32[512,512]{1,0:T(8,128)}, u32[]{:S(2)}) copy-start(f32[512,512]{1,0:T(8,128)} %qw.1) | copy-start | bytes 3145732

commit v8 on v6

--- a/solution.py
+++ b/solution.py
@@ -481,8 +481,8 @@
     gather_dirs(0)
     send_norms(0)
     spread_zs()
+    gather_dirs(3)
     spread_sums()
-    gather_dirs(3)
     send_norms(1)
     finish(0)
     finish(1)

time: 49.1 us -> 49.1 us (level)
  no operation moved by 1% of the time
where the time goes in v8:
time: 49.1 us; the launch traced here: 49 us
  Pallas kernels  48.2 us (98%)
  between operations  0.71 us (1%)
    pallas_call x1, Pallas kernels, on_device_fast(): pl.pallas_call(exchange_kernel, out_shape=(jax.ShapeDtypeStruct((2, 4, sh...  45.3 us
    pallas_call x1, Pallas kernels, on_device_fast(): pl.pallas_call(functools.partial(finish_kernel, entries), grid=(n,), out_...  2.94 us

profile of v8, /device:TPU:0, one launch (start us, length us, event | category | flops | bytes accessed | tf_op | source)
XLA Modules:
  0.0 49.0 jit_solution(16796007315708036249)
XLA Ops:
  0.6 0.0 copy-start.1
  0.6 0.0 copy-start
  0.7 0.0 copy-start.3
  0.7 0.0 copy-start.2
  0.7 45.3 %shard_map.161 = (bf16[2,4,128,512]{3,2,1,0:T(8,128)(2,1)S(1)}, f32[2,128,512]{2,1,0:T(8,128)S(1)}, f32[2,8,128]{2,1,0:T(8,128)S(1)}) custom-call(bf16[352,2048]{1,0:T(8,128)(2,1)} %si_hbm.1, bf16[352,2048]{1,0:T(8,128)(2,1)} %oc_hbm.1, bf16[352,512]{1,0:T(8,128)(2,1)} %qc_hbm.1, bf16[352,512]{1,0:T(8,128)(2,1)} %ao_hbm.1, bf16[512,512]{1,0:T(8,128)(2,1)} %qb.1, ...), custom_call_target="tpu_custom_call" | custom-call | tf_op jit(solution)/shard_map/pallas_call | solution.py:564
  46.0 0.0 copy-done.1
  46.0 0.0 copy-done
  46.0 0.0 copy-done.3
  46.0 0.0 copy-done.2
  46.0 2.9 %shard_map.162 = (f32[512,512]{1,0:T(8,128)}, f32[512,512]{1,0:T(8,128)}, f32[512,512]{1,0:T(8,128)}, f32[512,512]{1,0:T(8,128)}, bf16[512,512]{1,0:T(8,128)(2,1...) custom-call(bf16[512,512]{1,0:T(8,128)(2,1)S(1)} %copy-done, bf16[512,512]{1,0:T(8,128)(2,1)S(1)} %copy-done.1, ...), custom_call_target="tpu_custom_call" | custom-call | flops 536870912 | bytes 5242880 | tf_op jit(solution)/shard_map/pallas_call | solution.py:608
Async XLA Ops:
  0.6 45.4 %copy-start.1 = (bf16[512,512]{1,0:T(8,128)(2,1)S(1)}, bf16[512,512]{1,0:T(8,128)(2,1)}, u32[]{:S(2)}) copy-start(bf16[512,512]{1,0:T(8,128)(2,1)} %ob.1) | copy-start | bytes 1572868
  0.6 45.4 %copy-start = (bf16[512,512]{1,0:T(8,128)(2,1)S(1)}, bf16[512,512]{1,0:T(8,128)(2,1)}, u32[]{:S(2)}) copy-start(bf16[512,512]{1,0:T(8,128)(2,1)} %qb.1) | copy-start | bytes 1572868
  0.7 45.4 %copy-start.3 = (f32[512,512]{1,0:T(8,128)S(1)}, f32[512,512]{1,0:T(8,128)}, u32[]{:S(2)}) copy-start(f32[512,512]{1,0:T(8,128)} %ow.1) | copy-start | bytes 3145732
  0.7 45.4 %copy-start.2 = (f32[512,512]{1,0:T(8,128)S(1)}, f32[512,512]{1,0:T(8,128)}, u32[]{:S(2)}) copy-start(f32[512,512]{1,0:T(8,128)} %qw.1) | copy-start | bytes 3145732
